TPU v7x, 32 devices: a whole 2x2x4 slice. The times are simulated.
32 devices in a mesh: sp: 16 (over z, y, x), dp: 2 (over core).
Axes of the slice: x: 2, y: 2, z: 4, core: 2. Of those that a mesh axis runs over, the one named last changes fastest.
Arguments:
- inputs: bfloat16 [2, 2048, 2048], P('dp', 'sp'), may hold values from -6 to 6
- conv_weight: bfloat16 [4, 2048], replicated, may hold values from -3 to 3
- gate_weight: bfloat16 [2, 8, 256, 256], P(None, 'dp'), may hold values from -0.375 to 0.375
- rate_param: float32 [2048], replicated, may hold values from 4 to 12.5
- pace: float32 [2, 2048], P('dp'), may hold values from 0.5 to 30000
Outputs:
- recurrent: bfloat16 [2, 2048, 2048], P('dp', 'sp')
All inputs are finite; a program needn't handle non-finite values.
Results may differ from a plain program's by a relative error of at most 0.008.
Values may be sent and summed in bfloat16 or wider, within the bound.
A program may use at most 128 MiB of HBM per device.

v0:
```python
import functools
import math

import jax
import jax.numpy as jnp
from jax import lax
from jax.experimental import pallas as pl
from jax.experimental.pallas import tpu as pltpu
from jax.sharding import PartitionSpec as P

CONV = 4
EDGE = CONV - 1
gate_power = 8.0
SUB = 8
LANES = 128
PIECE = SUB * LANES
TINY = 1.2e-38
LN2 = math.log(2.0)
SMALL = 0.015
SPLIT = 2
FIRST = 1
NEAR = 4
MESH = pl.DeviceIdType.MESH


def softplus_neg(rate):
    e = jnp.exp(-jnp.abs(rate))
    series = e * (1.0 + e * (-0.5 + e * (1.0 / 3.0 + e * (-0.25 + e * 0.2))))
    return jnp.maximum(-rate, 0.0) + jnp.where(e < 0.03, series, jnp.log(1.0 + e))


def kernel(
    nsp, ndp, heads, block,
    x_hbm, cw_hbm, w_hbm, rate_hbm, pace_hbm, out_ref,
    x, cw, w, rate, pace_row, pace_mat, pace_perm, halo,
    ends, hloc, acum, ex_h, ex_a, stage, send_buf, recv_buf, carry,
    known, load_sem, map_sem, w_send, w_recv, halo_send, halo_recv, c_send, c_recv,
):
    me = lax.axis_index("sp")
    d = lax.axis_index("dp")
    count, width = x.shape
    steps = count // SUB
    hl = heads // ndp
    pieces = width // PIECE
    per = PIECE // block
    tiles = block // LANES

    barrier = pltpu.get_barrier_semaphore()

    def at_distance(delta, ahead, then):
        there = me + delta if ahead else me - delta

        @pl.when(there < nsp if ahead else there >= 0)
        def _():
            then(there)

    def greet(there):
        pl.semaphore_signal(barrier, inc=1, device_id={"sp": there}, device_id_type=MESH)

    near = range(1, min(NEAR, nsp - 1) + 1)
    for delta in near:
        for ahead in (True, False):
            at_distance(delta, ahead, greet)

    @pl.loop(1, ndp)
    def _(o):
        pl.semaphore_signal(barrier, inc=1, device_id={"dp": lax.rem(d + o, ndp)}, device_id_type=MESH)

    first = pl.multiple_of(me * count, count)
    loads = [
        pltpu.make_async_copy(x_hbm.at[0], x, load_sem.at[0]),
        pltpu.make_async_copy(cw_hbm, cw, load_sem.at[1]),
        pltpu.make_async_copy(rate_hbm, rate, load_sem.at[2]),
        pltpu.make_async_copy(pace_hbm.at[:, pl.ds(first, count)], pace_row, load_sem.at[3]),
    ]
    map_loads = [
        pltpu.make_async_copy(w_hbm.at[:, own], w.at[:, own], map_sem.at[own])
        for own in range(hl)
    ]
    for load in loads + map_loads:
        load.start()

    @pl.when(me == 0)
    def _():
        halo[...] = jnp.zeros_like(halo)

    rounds = []
    while NEAR * 2 ** len(rounds) < nsp - 1:
        rounds.append(NEAR * 2 ** len(rounds))

    def tell(n):
        for ahead in (True, False):
            at_distance(rounds[n], ahead, lambda there, ahead=ahead: pl.semaphore_signal(
                known.at[n, int(ahead)], inc=1, device_id={"sp": there}, device_id_type=MESH))

    def learn(n):
        for ahead in (True, False):
            at_distance(rounds[n], ahead, lambda _, ahead=ahead: pl.semaphore_wait(
                known.at[n, int(not ahead)], 1))

    w_copies = []
    for slot in range(hl, heads):
        o, own = slot // hl, slot % hl
        w_copies.append(pltpu.make_async_remote_copy(
            src_ref=w.at[:, own],
            dst_ref=w.at[:, slot],
            send_sem=w_send.at[slot],
            recv_sem=w_recv.at[slot],
            device_id={"dp": lax.rem(d - o + ndp, ndp)},
            device_id_type=MESH,
        ))
    halo_copy = pltpu.make_async_remote_copy(
        src_ref=x.at[pl.ds(count - SUB, SUB)],
        dst_ref=halo,
        send_sem=halo_send.at[0],
        recv_sem=halo_recv.at[0],
        device_id={"sp": lax.rem(me + 1, nsp)},
        device_id_type=MESH,
    )
    for load in loads:
        load.wait()

    def meet_and_send():
        reach = len(near)
        peers = jnp.minimum(me, reach) + jnp.minimum(nsp - 1 - me, reach)
        pl.semaphore_wait(barrier, peers + ndp - 1)

        @pl.when(me < nsp - 1)
        def _():
            halo_copy.start()

        for copy in w_copies:
            copy.start()
        if rounds:
            tell(0)

    spread = jnp.broadcast_to(pace_row[...], (LANES, count)).T
    pace_mat[...] = spread
    for j in range(steps):
        pace_perm[j] = pace_mat[pl.ds(j, SUB, stride=steps), :]

    row = lax.broadcasted_iota(jnp.int32, (count, count), 0)
    col = lax.broadcasted_iota(jnp.int32, (count, count), 1)
    gather = jnp.where(col == (row % SUB) * steps + row // SUB, 1.0, 0.0).astype(jnp.bfloat16)
    scatter = jnp.where(row == (col % SUB) * steps + col // SUB, 1.0, 0.0).astype(jnp.bfloat16)
    sub = lax.broadcasted_iota(jnp.int32, (SUB, block), 0)

    def carry_copy(piece, src, dst):
        return pltpu.make_async_remote_copy(
            src_ref=send_buf.at[piece],
            dst_ref=recv_buf.at[src, piece],
            send_sem=c_send.at[dst, piece],
            recv_sem=c_recv.at[src, piece],
            device_id={"sp": dst},
            device_id_type=MESH,
        )

    def take_halo():
        @pl.when(me > 0)
        def _():
            halo_copy.wait_recv()

    def columns(slot):
        return pl.ds(pl.multiple_of(lax.rem(d * hl + slot, heads) * block, block), block)

    def convolve(rows, here):
        taps = cw[:, here].astype(jnp.float32)
        taps = [jnp.broadcast_to(taps[k : k + 1], (SUB, block)) for k in range(CONV)]
        out = []
        for j in range(len(rows) - EDGE):
            total = taps[0] * rows[j]
            for k in range(1, CONV):
                total = total + taps[k] * rows[j + k]
            out.append(total)
        return out

    def terms(conv, slot, here, first_step):
        conv = jnp.concatenate(conv, axis=0).astype(jnp.bfloat16)
        pre_r = jnp.dot(conv, w[0, slot], preferred_element_type=jnp.float32)
        pre_i = jnp.dot(conv, w[1, slot], preferred_element_type=jnp.float32)
        values = conv.astype(jnp.float32)
        factor = softplus_neg(rate[:, here]) * (gate_power / LN2)
        factor = jnp.broadcast_to(factor, (SUB, block))
        for j in range(conv.shape[0] // SUB):
            part = slice(SUB * j, SUB * (j + 1))
            pace_j = jnp.concatenate([pace_perm[first_step + j]] * tiles, axis=1)
            r = 1.0 / (1.0 + jnp.exp(-pre_r[part]))
            i = 1.0 / (1.0 + jnp.exp(-pre_i[part]))
            q = pace_j * factor * r
            a = jnp.exp2(-q)
            c = 2.0 * LN2
            series = q * (c + q * (c**3 / 6 * q - c * c / 2))
            gain = jnp.where(q < SMALL, series, 1.0 - a * a)
            b = gain * lax.rsqrt(jnp.maximum(gain, TINY)) * i * values[part]
            yield a, b

    def scan(pairs, slot, first_step):
        h = total_a = None
        for j, (a, b) in enumerate(pairs, first_step):
            if h is None:
                h, total_a = b, a
            else:
                h = a * h + b
                total_a = total_a * a
            part = slice(SUB * j, SUB * (j + 1))
            hloc[slot, part] = h
            acum[slot, part] = total_a

    def main_slot(slot):
        here = columns(slot)
        xp = jnp.dot(gather, x[:, here], preferred_element_type=jnp.float32)
        rows = [xp[SUB * j : SUB * (j + 1)] for j in range(steps)]
        ends[slot] = jnp.concatenate(rows[steps - EDGE :] + rows[:EDGE], axis=0)
        scan(terms(convolve(rows, here), slot, here, EDGE), slot, EDGE)

    def with_halo(rows, here):
        before = halo[:, here].astype(jnp.float32)
        out = []
        for j in range(EDGE):
            edge = before[SUB - EDGE + j : SUB - EDGE + j + 1]
            out.append(jnp.where(sub == 0, jnp.broadcast_to(edge, (SUB, block)), pltpu.roll(rows[j], 1, 0)))
        return out

    def full_slot(piece, at):
        slot = piece * per + at
        here = columns(slot)
        xp = jnp.dot(gather, x[:, here], preferred_element_type=jnp.float32)
        rows = [xp[SUB * j : SUB * (j + 1)] for j in range(steps)]
        rows = with_halo(rows[steps - EDGE :], here) + rows
        scan(terms(convolve(rows, here), slot, here, 0), slot, 0)
        chunk_end = slice(SUB * (steps - 1), SUB * steps)
        totals(slot, at, hloc[slot, chunk_end], acum[slot, chunk_end])

    def edge_slot(piece, at):
        slot = piece * per + at
        here = columns(slot)
        rows = [ends[slot, SUB * j : SUB * (j + 1)] for j in range(2 * EDGE)]
        rows = with_halo(rows[:EDGE], here) + rows[EDGE:]
        conv = convolve(rows, here)
        scan(terms(conv, slot, here, 0), slot, 0)
        edge_end = slice(SUB * (EDGE - 1), SUB * EDGE)
        chunk_end = slice(SUB * (steps - 1), SUB * steps)
        h = hloc[slot, chunk_end] + acum[slot, chunk_end] * hloc[slot, edge_end]
        totals(slot, at, h, acum[slot, chunk_end] * acum[slot, edge_end])

    def totals(slot, at, h, total_a):
        for shift in (1, 2, 4):
            inside = sub >= shift
            earlier_a = jnp.where(inside, pltpu.roll(total_a, shift, 0), 1.0)
            earlier_h = jnp.where(inside, pltpu.roll(h, shift, 0), 0.0)
            h = total_a * earlier_h + h
            total_a = total_a * earlier_a
        ex_h[slot] = jnp.where(sub >= 1, pltpu.roll(h, 1, 0), 0.0)
        ex_a[slot] = jnp.where(sub >= 1, pltpu.roll(total_a, 1, 0), 1.0)
        log_a = jnp.log2(jnp.maximum(total_a, TINY))
        for t in range(tiles):
            lanes = slice(LANES * t, LANES * (t + 1))
            stage[pl.ds(at * tiles + t, 1), :] = log_a[SUB - 1 :, lanes]
            stage[pl.ds(SUB + at * tiles + t, 1), :] = h[SUB - 1 :, lanes]

    def wait_maps(low, high):
        for slot in range(max(hl, low), high):
            w_copies[slot - hl].wait_recv()

    def main_slots(low, high):
        wait_maps(low, high)

        @pl.loop(low, high, unroll=True)
        def _(slot):
            main_slot(slot)

    def edge_and_send(piece, split):
        @pl.loop(0, split, unroll=True)
        def _(at):
            edge_slot(piece, at)

        if split < per:
            wait_maps(piece * per + split, piece * per + per)

            @pl.loop(split, per, unroll=True)
            def _(at):
                full_slot(piece, at)

        send_buf[piece] = stage[...].astype(jnp.bfloat16)

        if piece == 0 and rounds:
            learn(len(rounds) - 1)

        @pl.loop(me + 1, nsp)
        def _(dst):
            carry_copy(piece, me, dst).start()

    half = per // 2
    for piece in range(pieces):
        low = piece * per
        if piece == 0:
            begun = low + min(hl, FIRST)
            for load in map_loads[:begun]:
                load.wait()
            middle = begun + (low + per - begun) // 2
            main_slots(low, begun)
            for load in map_loads[begun:]:
                load.wait()
            meet_and_send()
            main_slots(begun, middle)
            for n in range(1, len(rounds)):
                learn(n - 1)
                tell(n)
            main_slots(middle, low + per)
        else:
            ahead = SPLIT if piece == 1 else 0
            if ahead:
                main_slots(low, low + ahead)
            if piece == 1:
                take_halo()
                edge_and_send(0, per)
            edge_and_send(piece, ahead)

    def finish_slot(piece, at):
        slot = piece * per + at
        off = pl.multiple_of(lax.rem(d * hl + slot, heads) * block, block)
        start = jnp.concatenate(
            [
                jnp.broadcast_to(carry[pl.ds(at * tiles + t, 1), :], (SUB, LANES))
                for t in range(tiles)
            ],
            axis=1,
        )
        start = ex_h[slot] + ex_a[slot] * start
        edge_end = slice(SUB * (EDGE - 1), SUB * EDGE)
        later = start
        if piece == 0 or at < SPLIT:
            later = hloc[slot, edge_end] + acum[slot, edge_end] * start
        states = [
            hloc[slot, SUB * j : SUB * (j + 1)]
            + acum[slot, SUB * j : SUB * (j + 1)] * (start if j < EDGE else later)
            for j in range(steps)
        ]
        states = jnp.concatenate(states, axis=0).astype(jnp.bfloat16)
        placed = jnp.dot(scatter, states, preferred_element_type=jnp.float32)
        out_ref[0, :, pl.ds(off, block)] = placed.astype(jnp.bfloat16)

    for piece in range(pieces):
        carry[...] = jnp.zeros_like(carry)

        @pl.loop(0, me)
        def _(src):
            carry_copy(piece, src, me).wait_recv()
            got = recv_buf[src, piece].astype(jnp.float32)
            carry[...] = jnp.exp2(got[:SUB]) * carry[...] + got[SUB:]

        for at in range(per):
            finish_slot(piece, at)

    for copy in w_copies:
        copy.wait_send()

    @pl.when(me < nsp - 1)
    def _():
        halo_copy.wait_send()

    for piece in range(pieces):

        @pl.loop(me + 1, nsp)
        def _(dst):
            carry_copy(piece, me, dst).wait_send()


def body(inputs, conv_weight, gate_weight, rate_param, pace):
    nsp = lax.axis_size("sp")
    ndp = lax.axis_size("dp")
    _, count, width = inputs.shape
    block = gate_weight.shape[-1]
    heads = width // block
    hl = heads // ndp
    pieces = width // PIECE
    f32, bf16 = jnp.float32, jnp.bfloat16
    hbm = pl.BlockSpec(memory_space=pltpu.HBM)
    dma = pltpu.SemaphoreType.DMA
    return pl.pallas_call(
        functools.partial(kernel, nsp, ndp, heads, block),
        out_shape=pltpu.VMEM(inputs.shape, bf16),
        in_specs=[hbm] * 5,
        out_specs=pl.BlockSpec(memory_space=pltpu.VMEM),
        scratch_shapes=[
            pltpu.VMEM((count, width), bf16),
            pltpu.VMEM(conv_weight.shape, bf16),
            pltpu.VMEM((2, heads, block, block), bf16),
            pltpu.VMEM((1, width), f32),
            pltpu.VMEM((1, count), f32),
            pltpu.VMEM((count, LANES), f32),
            pltpu.VMEM((count // SUB, SUB, LANES), f32),
            pltpu.VMEM((SUB, width), bf16),
            pltpu.VMEM((heads, 2 * EDGE * SUB, block), f32),
            pltpu.VMEM((heads, count, block), f32),
            pltpu.VMEM((heads, count, block), f32),
            pltpu.VMEM((heads, SUB, block), f32),
            pltpu.VMEM((heads, SUB, block), f32),
            pltpu.VMEM((2 * SUB, LANES), f32),
            pltpu.VMEM((pieces, 2 * SUB, LANES), bf16),
            pltpu.VMEM((nsp, pieces, 2 * SUB, LANES), bf16),
            pltpu.VMEM((SUB, LANES), f32),
            pltpu.SemaphoreType.REGULAR((8, 2)),
            dma((4,)),
            dma((hl,)),
            dma((heads,)),
            dma((heads,)),
            dma((1,)),
            dma((1,)),
            dma((nsp, pieces)),
            dma((nsp, pieces)),
        ],
        compiler_params=pltpu.CompilerParams(collective_id=0, has_side_effects=True),
    )(inputs, conv_weight, gate_weight, rate_param.reshape(1, width), pace)


def solution(mesh):
    return jax.shard_map(
        body,
        mesh=mesh,
        in_specs=(P("dp", "sp", None), P(), P(None, "dp", None, None), P(), P("dp", None)),
        out_specs=P("dp", "sp", None),
        check_vma=False,
    )
```

profile of v0, /device:TPU:16, one launch (start us, length us, event | category | flops | bytes accessed | tf_op | source)
XLA Modules:
  0.0 13.0 jit_solution(13319885940097721536)
XLA Ops:
  0.0 12.2 %shard_map.55 = bf16[1,128,2048]{2,1,0:T(8,128)(2,1)S(1)} custom-call(bf16[1,128,2048]{2,1,0:T(8,128)(2,1)} %x_hbm.1, bf16[4,2048]{1,0:T(4,128)(2,1)} %cw_hbm.1, bf16[2,4,256,256]{3,2,1,0:T(8,128)(2,1)} %w_hbm.1, f32[1,2048]{1,0:T(1,128)} %bitcast.1, f32[1,2048]{1,0:T(1,128)} %pace_hbm.1), custom_call_target="tpu_custom_call" | custom-call | tf_op jit(solution)/shard_map/pallas_call | solution.py:380
  12.2 0.8 %copy.7 = bf16[1,128,2048]{2,1,0:T(8,128)(2,1)} copy(bf16[1,128,2048]{2,1,0:T(8,128)(2,1)S(1)} %shard_map.55) | data formatting | bytes 1048576
where the time goes:
time: 13.2 us; the launch traced here: 13 us
  Pallas kernels  12.2 us (92%)
  local copies, waits for them, and re-layouts  0.8 us (6%)
    pallas_call x1, Pallas kernels, body(): pl.pallas_call(functools.partial(kernel, nsp, ndp, heads, block), out_sha...  12.2 us
    unnamed x1, local copies, waits for them, and re-layouts  0.8 us

commit v1 on v0

--- a/solution.py
+++ b/solution.py
@@ -19,7 +19,6 @@
 SMALL = 0.015
 SPLIT = 2
 FIRST = 1
-NEAR = 4
 MESH = pl.DeviceIdType.MESH
 
 
@@ -45,58 +44,85 @@
     per = PIECE // block
     tiles = block // LANES
 
-    barrier = pltpu.get_barrier_semaphore()
-
-    def at_distance(delta, ahead, then):
-        there = me + delta if ahead else me - delta
-
-        @pl.when(there < nsp if ahead else there >= 0)
-        def _():
-            then(there)
-
-    def greet(there):
-        pl.semaphore_signal(barrier, inc=1, device_id={"sp": there}, device_id_type=MESH)
-
-    near = range(1, min(NEAR, nsp - 1) + 1)
-    for delta in near:
-        for ahead in (True, False):
-            at_distance(delta, ahead, greet)
-
-    @pl.loop(1, ndp)
-    def _(o):
-        pl.semaphore_signal(barrier, inc=1, device_id={"dp": lax.rem(d + o, ndp)}, device_id_type=MESH)
-
+    root = nsp - 1
     first = pl.multiple_of(me * count, count)
     loads = [
-        pltpu.make_async_copy(x_hbm.at[0], x, load_sem.at[0]),
-        pltpu.make_async_copy(cw_hbm, cw, load_sem.at[1]),
-        pltpu.make_async_copy(rate_hbm, rate, load_sem.at[2]),
-        pltpu.make_async_copy(pace_hbm.at[:, pl.ds(first, count)], pace_row, load_sem.at[3]),
+        pltpu.make_async_copy(x_hbm.at[0], x, load_sem),
+        pltpu.make_async_copy(cw_hbm, cw, load_sem),
+        pltpu.make_async_copy(rate_hbm, rate, load_sem),
+        pltpu.make_async_copy(pace_hbm.at[:, pl.ds(first, count)], pace_row, load_sem),
     ]
     map_loads = [
-        pltpu.make_async_copy(w_hbm.at[:, own], w.at[:, own], map_sem.at[own])
+        pltpu.make_async_copy(w_hbm.at[:, own], w.at[:, own], map_sem.at[int(own >= FIRST)])
         for own in range(hl)
     ]
     for load in loads + map_loads:
         load.start()
 
+    recv_buf[...] = jnp.zeros_like(recv_buf)
+
+    barrier = pltpu.get_barrier_semaphore()
+
+    def greet(there):
+        pl.semaphore_signal(barrier, inc=1, device_id={"sp": there}, device_id_type=MESH)
+
+    @pl.loop(1, ndp)
+    def _(o):
+        pl.semaphore_signal(barrier, inc=1, device_id={"dp": lax.rem(d + o, ndp)}, device_id_type=MESH)
+
+    if root > 0:
+
+        @pl.when(me < root)
+        def _():
+            greet(root)
+
+    if root > 1:
+
+        @pl.when(me >= 2)
+        def _():
+            greet(me - 1)
+
+        @pl.when(me == 0)
+        def _():
+            greet(1)
+
     @pl.when(me == 0)
     def _():
         halo[...] = jnp.zeros_like(halo)
 
-    rounds = []
-    while NEAR * 2 ** len(rounds) < nsp - 1:
-        rounds.append(NEAR * 2 ** len(rounds))
-
-    def tell(n):
-        for ahead in (True, False):
-            at_distance(rounds[n], ahead, lambda there, ahead=ahead: pl.semaphore_signal(
-                known.at[n, int(ahead)], inc=1, device_id={"sp": there}, device_id_type=MESH))
-
-    def learn(n):
-        for ahead in (True, False):
-            at_distance(rounds[n], ahead, lambda _, ahead=ahead: pl.semaphore_wait(
-                known.at[n, int(not ahead)], 1))
+    def tell(which, there):
+        pl.semaphore_signal(known.at[which], inc=1, device_id={"sp": there}, device_id_type=MESH)
+
+    def meet_early():
+        if root > 0:
+
+            @pl.when(me == root)
+            def _():
+                pl.semaphore_wait(barrier, ndp - 1 + root)
+                for there in range(root):
+                    tell(0, there)
+
+            @pl.when(me == 1)
+            def _():
+                if root > 1:
+                    pl.semaphore_wait(barrier, ndp - 1 + 2)
+                tell(1, 0)
+
+    def meet():
+        if root == 0:
+            pl.semaphore_wait(barrier, ndp - 1)
+        else:
+
+            @pl.when(jnp.logical_and(me != root, me != 1))
+            def _():
+                pl.semaphore_wait(barrier, ndp - 1 + jnp.minimum(me, 1))
+
+    def all_in():
+        if root > 0:
+
+            @pl.when(me < root)
+            def _():
+                pl.semaphore_wait(known.at[0], 1)
 
     w_copies = []
     for slot in range(hl, heads):
@@ -104,35 +130,42 @@
         w_copies.append(pltpu.make_async_remote_copy(
             src_ref=w.at[:, own],
             dst_ref=w.at[:, slot],
-            send_sem=w_send.at[slot],
-            recv_sem=w_recv.at[slot],
+            send_sem=w_send,
+            recv_sem=w_recv.at[slot - hl],
             device_id={"dp": lax.rem(d - o + ndp, ndp)},
             device_id_type=MESH,
         ))
     halo_copy = pltpu.make_async_remote_copy(
         src_ref=x.at[pl.ds(count - SUB, SUB)],
         dst_ref=halo,
-        send_sem=halo_send.at[0],
-        recv_sem=halo_recv.at[0],
+        send_sem=halo_send,
+        recv_sem=halo_recv,
         device_id={"sp": lax.rem(me + 1, nsp)},
         device_id_type=MESH,
     )
+    meet_early()
     for load in loads:
         load.wait()
 
     def meet_and_send():
-        reach = len(near)
-        peers = jnp.minimum(me, reach) + jnp.minimum(nsp - 1 - me, reach)
-        pl.semaphore_wait(barrier, peers + ndp - 1)
-
-        @pl.when(me < nsp - 1)
-        def _():
-            halo_copy.start()
+        meet()
+
+        if root > 0:
+
+            @pl.when(jnp.logical_and(me > 0, me < root))
+            def _():
+                halo_copy.start()
 
         for copy in w_copies:
             copy.start()
-        if rounds:
-            tell(0)
+
+    def first_halo():
+        if root > 0:
+
+            @pl.when(me == 0)
+            def _():
+                pl.semaphore_wait(known.at[1], 1)
+                halo_copy.start()
 
     spread = jnp.broadcast_to(pace_row[...], (LANES, count)).T
     pace_mat[...] = spread
@@ -148,10 +181,21 @@
     def carry_copy(piece, src, dst):
         return pltpu.make_async_remote_copy(
             src_ref=send_buf.at[piece],
-            dst_ref=recv_buf.at[src, piece],
-            send_sem=c_send.at[dst, piece],
-            recv_sem=c_recv.at[src, piece],
+            dst_ref=recv_buf.at[piece, src],
+            send_sem=c_send.at[piece],
+            recv_sem=c_recv.at[piece],
             device_id={"sp": dst},
+            device_id_type=MESH,
+        )
+
+    def carries(piece, many):
+        block = recv_buf.at[piece, pl.ds(0, many)]
+        return pltpu.make_async_remote_copy(
+            src_ref=block,
+            dst_ref=block,
+            send_sem=c_send.at[piece],
+            recv_sem=c_recv.at[piece],
+            device_id={"sp": root - me},
             device_id_type=MESH,
         )
 
@@ -283,8 +327,8 @@
 
         send_buf[piece] = stage[...].astype(jnp.bfloat16)
 
-        if piece == 0 and rounds:
-            learn(len(rounds) - 1)
+        if piece == 0:
+            all_in()
 
         @pl.loop(me + 1, nsp)
         def _(dst):
@@ -303,9 +347,7 @@
                 load.wait()
             meet_and_send()
             main_slots(begun, middle)
-            for n in range(1, len(rounds)):
-                learn(n - 1)
-                tell(n)
+            first_halo()
             main_slots(middle, low + per)
         else:
             ahead = SPLIT if piece == 1 else 0
@@ -341,13 +383,18 @@
         out_ref[0, :, pl.ds(off, block)] = placed.astype(jnp.bfloat16)
 
     for piece in range(pieces):
-        carry[...] = jnp.zeros_like(carry)
-
-        @pl.loop(0, me)
-        def _(src):
-            carry_copy(piece, src, me).wait_recv()
-            got = recv_buf[src, piece].astype(jnp.float32)
-            carry[...] = jnp.exp2(got[:SUB]) * carry[...] + got[SUB:]
+
+        for many in range(1, nsp):
+
+            @pl.when(me == many)
+            def _(many=many):
+                carries(piece, many).wait_recv()
+
+        start = jnp.zeros(carry.shape, jnp.float32)
+        for src in range(root):
+            got = recv_buf[piece, src].astype(jnp.float32)
+            start = jnp.exp2(got[:SUB]) * start + got[SUB:]
+        carry[...] = start
 
         for at in range(per):
             finish_slot(piece, at)
@@ -361,9 +408,11 @@
 
     for piece in range(pieces):
 
-        @pl.loop(me + 1, nsp)
-        def _(dst):
-            carry_copy(piece, me, dst).wait_send()
+        for many in range(1, nsp):
+
+            @pl.when(root - me == many)
+            def _(many=many):
+                carries(piece, many).wait_send()
 
 
 def body(inputs, conv_weight, gate_weight, rate_param, pace):
@@ -398,17 +447,17 @@
             pltpu.VMEM((heads, SUB, block), f32),
             pltpu.VMEM((2 * SUB, LANES), f32),
             pltpu.VMEM((pieces, 2 * SUB, LANES), bf16),
-            pltpu.VMEM((nsp, pieces, 2 * SUB, LANES), bf16),
+            pltpu.VMEM((pieces, nsp, 2 * SUB, LANES), bf16),
             pltpu.VMEM((SUB, LANES), f32),
-            pltpu.SemaphoreType.REGULAR((8, 2)),
-            dma((4,)),
-            dma((hl,)),
-            dma((heads,)),
-            dma((heads,)),
-            dma((1,)),
-            dma((1,)),
-            dma((nsp, pieces)),
-            dma((nsp, pieces)),
+            pltpu.SemaphoreType.REGULAR((2,)),
+            dma,
+            dma((2,)),
+            dma,
+            dma((heads - hl,)),
+            dma,
+            dma,
+            dma((pieces,)),
+            dma((pieces,)),
         ],
         compiler_params=pltpu.CompilerParams(collective_id=0, has_side_effects=True),
     )(inputs, conv_weight, gate_weight, rate_param.reshape(1, width), pace)

time: 13.2 us -> 11.7 us (0.89)
  the two profiles are of different devices: /device:TPU:16 before, /device:TPU:24 now
where the time goes in v1:
time: 11.7 us; the launch traced here: 11.5 us
  Pallas kernels  10.7 us (91%)
  local copies, waits for them, and re-layouts  0.8 us (7%)
    pallas_call x1, Pallas kernels, body(): pl.pallas_call(functools.partial(kernel, nsp, ndp, heads, block), out_sha...  10.7 us
    unnamed x1, local copies, waits for them, and re-layouts  0.8 us

profile of v1, /device:TPU:24, one launch (start us, length us, event | category | flops | bytes accessed | tf_op | source)
XLA Modules:
  0.0 11.5 jit_solution(17020938193507795677)
XLA Ops:
  0.0 10.7 %shard_map.55 = bf16[1,128,2048]{2,1,0:T(8,128)(2,1)S(1)} custom-call(bf16[1,128,2048]{2,1,0:T(8,128)(2,1)} %x_hbm.1, bf16[4,2048]{1,0:T(4,128)(2,1)} %cw_hbm.1, bf16[2,4,256,256]{3,2,1,0:T(8,128)(2,1)} %w_hbm.1, f32[1,2048]{1,0:T(1,128)} %bitcast.1, f32[1,2048]{1,0:T(1,128)} %pace_hbm.1), custom_call_target="tpu_custom_call" | custom-call | tf_op jit(solution)/shard_map/pallas_call | solution.py:429
  10.7 0.8 %copy.7 = bf16[1,128,2048]{2,1,0:T(8,128)(2,1)} copy(bf16[1,128,2048]{2,1,0:T(8,128)(2,1)S(1)} %shard_map.55) | data formatting | bytes 1048576

commit v2 on v1

v2 whole, which is shorter than its diff:
```python
import functools
import math

import jax
import jax.numpy as jnp
from jax import lax
from jax.experimental import pallas as pl
from jax.experimental.pallas import tpu as pltpu
from jax.sharding import PartitionSpec as P

CONV = 4
EDGE = CONV - 1
gate_power = 8.0
SUB = 8
LANES = 128
TINY = 1.2e-38
LN2 = math.log(2.0)
LOG2E = 1.0 / LN2
SMALL = 0.015
ROW = 4
FIRST = 2
MESH = pl.DeviceIdType.MESH


def softplus_neg(rate):
    e = jnp.exp(-jnp.abs(rate))
    series = e * (1.0 + e * (-0.5 + e * (1.0 / 3.0 + e * (-0.25 + e * 0.2))))
    return jnp.maximum(-rate, 0.0) + jnp.where(e < 0.03, series, jnp.log(1.0 + e))


def kernel(
    nsp, ndp, heads, block,
    x_hbm, cw_hbm, w_hbm, rate_hbm, pace_hbm, out_ref,
    x, cw, w, rate, pace_row, pace_mat, pace_perm, last, halo,
    ends, convs, hloc, acum, ex_h, ex_a, stage, send_buf, recv_buf, carry,
    known, met, load_sem, map_sem, w_send, w_recv, halo_send, halo_recv, c_send, c_recv,
):
    me = lax.axis_index("sp")
    d = lax.axis_index("dp")
    count, width = x.shape
    steps = count // SUB
    hl = heads // ndp
    tiles = block // LANES
    lines = heads * tiles
    root = nsp - 1
    scope = jax.named_scope

    first = pl.multiple_of(me * count, count)
    loads = [
        pltpu.make_async_copy(x_hbm.at[0], x, load_sem),
        pltpu.make_async_copy(cw_hbm, cw, load_sem),
        pltpu.make_async_copy(rate_hbm, rate, load_sem),
        pltpu.make_async_copy(pace_hbm.at[:, pl.ds(first, count)], pace_row, load_sem),
    ]
    map_loads = [
        pltpu.make_async_copy(w_hbm.at[:, own], w.at[:, own], map_sem.at[int(own >= FIRST)])
        for own in range(hl)
    ]
    for load in loads + map_loads:
        load.start()

    recv_buf[...] = jnp.zeros_like(recv_buf)

    barrier = pltpu.get_barrier_semaphore()

    def greet(there):
        pl.semaphore_signal(barrier, inc=1, device_id={"sp": there}, device_id_type=MESH)

    @pl.loop(d + 1, ndp)
    def _(o):
        pl.semaphore_signal(barrier, inc=1, device_id={"dp": o}, device_id_type=MESH)

    if root > 0:

        @pl.when(me > 0)
        def _():
            greet(me - 1)

    if root > 1:

        @pl.when(me < root - 1)
        def _():
            greet(root)

        @pl.when(me == root - 1)
        def _():
            greet(root)

    @pl.when(me == 0)
    def _():
        halo[...] = jnp.zeros_like(halo)

    def meet():
        pl.semaphore_wait(barrier, d + jnp.where(me == root, root if root > 1 else 0, min(root, 1)))

    def meet_early():
        if root > 0:

            @pl.when(me == root)
            def _():
                meet()
                for there in range(root):
                    pl.semaphore_signal(known, inc=1, device_id={"sp": there}, device_id_type=MESH)

    def meet_maps():
        @pl.when(jnp.logical_and(me < max(root, 1), d > 0))
        def _():
            meet()

        @pl.loop(0, d)
        def _(o):
            pl.semaphore_signal(met, inc=1, device_id={"dp": o}, device_id_type=MESH)

        @pl.when(d < ndp - 1)
        def _():
            pl.semaphore_wait(met, ndp - 1 - d)

    def meet_halo():
        @pl.when(jnp.logical_and(me < root, d == 0))
        def _():
            meet()

    w_copies = []
    for slot in range(hl, heads):
        o, own = slot // hl, slot % hl
        w_copies.append(pltpu.make_async_remote_copy(
            src_ref=w.at[:, own],
            dst_ref=w.at[:, slot],
            send_sem=w_send,
            recv_sem=w_recv.at[slot - hl],
            device_id={"dp": lax.rem(d - o + ndp, ndp)},
            device_id_type=MESH,
        ))
    halo_copy = pltpu.make_async_remote_copy(
        src_ref=last,
        dst_ref=halo,
        send_sem=halo_send,
        recv_sem=halo_recv,
        device_id={"sp": lax.rem(me + 1, nsp)},
        device_id_type=MESH,
    )

    def carry_copy(src, dst):
        return pltpu.make_async_remote_copy(
            src_ref=send_buf,
            dst_ref=recv_buf.at[src],
            send_sem=c_send,
            recv_sem=c_recv,
            device_id={"sp": dst},
            device_id_type=MESH,
        )

    def carries(many):
        block = recv_buf.at[pl.ds(0, many)]
        return pltpu.make_async_remote_copy(
            src_ref=block,
            dst_ref=block,
            send_sem=c_send,
            recv_sem=c_recv,
            device_id={"sp": root - me},
            device_id_type=MESH,
        )

    row = lax.broadcasted_iota(jnp.int32, (count, count), 0)
    col = lax.broadcasted_iota(jnp.int32, (count, count), 1)
    gather = jnp.where(col == (row % SUB) * steps + row // SUB, 1.0, 0.0).astype(jnp.bfloat16)
    scatter = jnp.where(row == (col % SUB) * steps + col // SUB, 1.0, 0.0).astype(jnp.bfloat16)
    sub = lax.broadcasted_iota(jnp.int32, (SUB, block), 0)

    def columns(slot):
        return pl.ds(pl.multiple_of(lax.rem(d * hl + slot, heads) * block, block), block)

    def convolve(rows, here):
        taps = cw[:, here].astype(jnp.float32)
        taps = [jnp.broadcast_to(taps[k : k + 1], (SUB, block)) for k in range(CONV)]
        out = []
        for j in range(len(rows) - EDGE):
            total = taps[0] * rows[j]
            for k in range(1, CONV):
                total = total + taps[k] * rows[j + k]
            out.append(total)
        return jnp.concatenate(out, axis=0)

    def conv_main(slot):
        here = columns(slot)
        xp = jnp.dot(gather, x[:, here], preferred_element_type=jnp.float32)
        rows = [xp[SUB * j : SUB * (j + 1)] for j in range(steps)]
        ends[slot] = jnp.concatenate(rows[steps - EDGE :] + rows[:EDGE], axis=0)
        convs[slot] = convolve(rows, here)

    def conv_edge(slot):
        here = columns(slot)
        rows = [ends[slot, SUB * j : SUB * (j + 1)] for j in range(2 * EDGE)]
        before = halo[:, here].astype(jnp.float32)
        for j in range(EDGE):
            edge = before[CONV - EDGE + j : CONV - EDGE + j + 1]
            rows[j] = jnp.where(sub == 0, jnp.broadcast_to(edge, (SUB, block)), pltpu.roll(rows[j], 1, 0))
        return convolve(rows, here)

    def scan(conv, slot, first_step):
        conv = conv.astype(jnp.bfloat16)
        pre_r = jnp.dot(conv, w[0, slot], preferred_element_type=jnp.float32)
        pre_i = jnp.dot(conv, w[1, slot], preferred_element_type=jnp.float32)
        values = conv.astype(jnp.float32)
        factor = softplus_neg(rate[:, columns(slot)]) * (-gate_power / LN2)
        factor = jnp.broadcast_to(factor, (SUB, block))
        h = total_a = None
        for j in range(conv.shape[0] // SUB):
            part = slice(SUB * j, SUB * (j + 1))
            pace_j = jnp.concatenate([pace_perm[first_step + j]] * tiles, axis=1)
            r = 1.0 / (1.0 + jnp.exp2(pre_r[part] * -LOG2E))
            i = 1.0 / (1.0 + jnp.exp2(pre_i[part] * -LOG2E))
            n = pace_j * factor * r
            a = jnp.exp2(n)
            c = 2.0 * LN2
            series = n * (n * (n * (-(c**3) / 6) - c * c / 2) - c)
            gain = jnp.where(n > -SMALL, series, 1.0 - a * a)
            b = gain * lax.rsqrt(jnp.maximum(gain, TINY)) * i * values[part]
            if h is None:
                h, total_a = b, a
            else:
                h = a * h + b
                total_a = total_a * a
            place = slice(SUB * (first_step + j), SUB * (first_step + j + 1))
            hloc[slot, place] = h
            acum[slot, place] = total_a

    def main_slot(slot):
        scan(convs[slot], slot, EDGE)

    def edge_slot(slot):
        scan(conv_edge(slot), slot, 0)
        edge_end = slice(SUB * (EDGE - 1), SUB * EDGE)
        chunk_end = slice(SUB * (steps - 1), SUB * steps)
        h = hloc[slot, chunk_end] + acum[slot, chunk_end] * hloc[slot, edge_end]
        totals(slot, h, acum[slot, chunk_end] * acum[slot, edge_end])

    def totals(slot, h, total_a):
        for shift in (1, 2, 4):
            inside = sub >= shift
            earlier_a = jnp.where(inside, pltpu.roll(total_a, shift, 0), 1.0)
            earlier_h = jnp.where(inside, pltpu.roll(h, shift, 0), 0.0)
            h = total_a * earlier_h + h
            total_a = total_a * earlier_a
        ex_h[slot] = jnp.where(sub >= 1, pltpu.roll(h, 1, 0), 0.0)
        ex_a[slot] = jnp.where(sub >= 1, pltpu.roll(total_a, 1, 0), 1.0)
        log_a = jnp.log2(jnp.maximum(total_a, TINY))
        for t in range(tiles):
            lanes = slice(LANES * t, LANES * (t + 1))
            stage[pl.ds(slot * tiles + t, 1), :] = log_a[SUB - 1 :, lanes]
            stage[pl.ds(lines + slot * tiles + t, 1), :] = h[SUB - 1 :, lanes]

    with scope("meet_early"):
        meet_early()
    with scope("loads"):
        for load in loads:
            load.wait()
    last[...] = x[count - SUB :, :].astype(jnp.float32)[SUB - CONV :].astype(jnp.bfloat16)
    with scope("meet_maps"):
        meet_maps()
    with scope("maps_a"):
        for load in map_loads[:FIRST]:
            load.wait()
        for own in range(min(FIRST, hl)):
            for copy in w_copies[own::hl]:
                copy.start()

    def send_halo():
        if root > 0:

            @pl.when(me < root)
            def _():
                halo_copy.start()

    @pl.when(d > 0)
    def _():
        send_halo()

    spread = jnp.broadcast_to(pace_row[...], (LANES, count)).T
    pace_mat[...] = spread
    for j in range(steps):
        pace_perm[j] = pace_mat[pl.ds(j, SUB, stride=steps), :]

    with scope("conv_own"):
        for slot in range(hl):
            conv_main(slot)
    with scope("maps_b"):
        for load in map_loads[FIRST:]:
            load.wait()
        for own in range(FIRST, hl):
            for copy in w_copies[own::hl]:
                copy.start()
    with scope("meet_halo"):
        meet_halo()

    @pl.when(d == 0)
    def _():
        send_halo()

    with scope("own"):
        for slot in range(hl):
            main_slot(slot)
        for slot in range(hl, heads):
            conv_main(slot)
    for slot in range(hl, heads):
        with scope("map%d" % slot):
            w_copies[slot - hl].wait_recv()
        with scope("main%d" % slot):
            main_slot(slot)
    with scope("take_halo"):

        @pl.when(me > 0)
        def _():
            halo_copy.wait_recv()

    with scope("edges"):
        for slot in range(heads):
            edge_slot(slot)
        send_buf[...] = stage[...].astype(jnp.bfloat16)
    with scope("all_in"):

        @pl.when(me < root)
        def _():
            pl.semaphore_wait(known, 1)

    for rest in range(ROW):
        for dst in range(nsp - ROW + rest, 0, -ROW):

            @pl.when(me < dst)
            def _(dst=dst):
                carry_copy(me, dst).start()

    with scope("carry"):
        for many in range(1, nsp):

            @pl.when(me == many)
            def _(many=many):
                carries(many).wait_recv()

    with scope("finish"):
        start = jnp.zeros(carry.shape, jnp.float32)
        for src in range(root):
            got = recv_buf[src].astype(jnp.float32)
            start = jnp.exp2(got[:lines]) * start + got[lines:]
        carry[...] = start

        for slot in range(heads):
            start = jnp.concatenate(
                [
                    jnp.broadcast_to(carry[pl.ds(slot * tiles + t, 1), :], (SUB, LANES))
                    for t in range(tiles)
                ],
                axis=1,
            )
            start = ex_h[slot] + ex_a[slot] * start
            edge_end = slice(SUB * (EDGE - 1), SUB * EDGE)
            later = hloc[slot, edge_end] + acum[slot, edge_end] * start
            states = [
                hloc[slot, SUB * j : SUB * (j + 1)]
                + acum[slot, SUB * j : SUB * (j + 1)] * (start if j < EDGE else later)
                for j in range(steps)
            ]
            states = jnp.concatenate(states, axis=0).astype(jnp.bfloat16)
            placed = jnp.dot(scatter, states, preferred_element_type=jnp.float32)
            out_ref[0, :, columns(slot)] = placed.astype(jnp.bfloat16)

    with scope("tail"):
        for copy in w_copies:
            copy.wait_send()

        if root > 0:

            @pl.when(me < root)
            def _():
                halo_copy.wait_send()

        for many in range(1, nsp):

            @pl.when(root - me == many)
            def _(many=many):
                carries(many).wait_send()


def body(inputs, conv_weight, gate_weight, rate_param, pace):
    nsp = lax.axis_size("sp")
    ndp = lax.axis_size("dp")
    _, count, width = inputs.shape
    block = gate_weight.shape[-1]
    heads = width // block
    hl = heads // ndp
    lines = width // LANES
    f32, bf16 = jnp.float32, jnp.bfloat16
    hbm = pl.BlockSpec(memory_space=pltpu.HBM)
    dma = pltpu.SemaphoreType.DMA
    return pl.pallas_call(
        functools.partial(kernel, nsp, ndp, heads, block),
        out_shape=pltpu.VMEM(inputs.shape, bf16),
        in_specs=[hbm] * 5,
        out_specs=pl.BlockSpec(memory_space=pltpu.VMEM),
        scratch_shapes=[
            pltpu.VMEM((count, width), bf16),
            pltpu.VMEM(conv_weight.shape, bf16),
            pltpu.VMEM((2, heads, block, block), bf16),
            pltpu.VMEM((1, width), f32),
            pltpu.VMEM((1, count), f32),
            pltpu.VMEM((count, LANES), f32),
            pltpu.VMEM((count // SUB, SUB, LANES), f32),
            pltpu.VMEM((CONV, width), bf16),
            pltpu.VMEM((CONV, width), bf16),
            pltpu.VMEM((heads, 2 * EDGE * SUB, block), f32),
            pltpu.VMEM((heads, count - EDGE * SUB, block), f32),
            pltpu.VMEM((heads, count, block), f32),
            pltpu.VMEM((heads, count, block), f32),
            pltpu.VMEM((heads, SUB, block), f32),
            pltpu.VMEM((heads, SUB, block), f32),
            pltpu.VMEM((2 * lines, LANES), f32),
            pltpu.VMEM((2 * lines, LANES), bf16),
            pltpu.VMEM((nsp, 2 * lines, LANES), bf16),
            pltpu.VMEM((lines, LANES), f32),
            pltpu.SemaphoreType.REGULAR,
            pltpu.SemaphoreType.REGULAR,
            dma,
            dma((2,)),
            dma,
            dma((heads - hl,)),
            dma,
            dma,
            dma,
            dma,
        ],
        compiler_params=pltpu.CompilerParams(collective_id=0, has_side_effects=True),
    )(inputs, conv_weight, gate_weight, rate_param.reshape(1, width), pace)


def solution(mesh):
    return jax.shard_map(
        body,
        mesh=mesh,
        in_specs=(P("dp", "sp", None), P(), P(None, "dp", None, None), P(), P("dp", None)),
        out_specs=P("dp", "sp", None),
        check_vma=False,
    )
```

time: 11.7 us -> 10.9 us (0.932)
  the two profiles are of different devices: /device:TPU:24 before, /device:TPU:16 now
where the time goes in v2:
time: 10.9 us; the launch traced here: 10.7 us
  Pallas kernels  9.94 us (91%)
  local copies, waits for them, and re-layouts  0.8 us (7%)
    pallas_call x1, Pallas kernels, body(): pl.pallas_call(functools.partial(kernel, nsp, ndp, heads, block), out_sha...  9.94 us
    unnamed x1, local copies, waits for them, and re-layouts  0.8 us

profile of v2, /device:TPU:16, one launch (start us, length us, event | category | flops | bytes accessed | tf_op | source)
XLA Modules:
  0.0 10.7 jit_solution(1443401827525742071)
XLA Ops:
  0.0 9.9 %shard_map.55 = bf16[1,128,2048]{2,1,0:T(8,128)(2,1)S(1)} custom-call(bf16[1,128,2048]{2,1,0:T(8,128)(2,1)} %x_hbm.1, bf16[4,2048]{1,0:T(4,128)(2,1)} %cw_hbm.1, bf16[2,4,256,256]{3,2,1,0:T(8,128)(2,1)} %w_hbm.1, f32[1,2048]{1,0:T(1,128)} %bitcast.1, f32[1,2048]{1,0:T(1,128)} %pace_hbm.1), custom_call_target="tpu_custom_call" | custom-call | tf_op jit(solution)/shard_map/pallas_call | solution.py:395
  9.9 0.8 %copy.7 = bf16[1,128,2048]{2,1,0:T(8,128)(2,1)} copy(bf16[1,128,2048]{2,1,0:T(8,128)(2,1)S(1)} %shard_map.55) | data formatting | bytes 1048576

commit v3 on v2

--- a/solution.py
+++ b/solution.py
@@ -30,9 +30,9 @@
 
 def kernel(
     nsp, ndp, heads, block,
-    x_hbm, cw_hbm, w_hbm, rate_hbm, pace_hbm, out_ref,
+    x_hbm, cw_hbm, w_hbm, rate_hbm, pace_hbm, part_h, part_a, carry,
     x, cw, w, rate, pace_row, pace_mat, pace_perm, last, halo,
-    ends, convs, hloc, acum, ex_h, ex_a, stage, send_buf, recv_buf, carry,
+    ends, convs, hloc, acum, ex_h, ex_a, lay_h, lay_a, stage, send_buf, recv_buf,
     known, met, load_sem, map_sem, w_send, w_recv, halo_send, halo_recv, c_send, c_recv,
 ):
     me = lax.axis_index("sp")
@@ -140,18 +140,18 @@
         device_id_type=MESH,
     )
 
-    def carry_copy(src, dst):
+    def carry_copy(src, dst, low=0):
         return pltpu.make_async_remote_copy(
-            src_ref=send_buf,
-            dst_ref=recv_buf.at[src],
+            src_ref=send_buf.at[pl.ds(low, 2 * lines - low)],
+            dst_ref=recv_buf.at[pl.ds(2 * lines * src + low, 2 * lines - low)],
             send_sem=c_send,
             recv_sem=c_recv,
             device_id={"sp": dst},
             device_id_type=MESH,
         )
 
-    def carries(many):
-        block = recv_buf.at[pl.ds(0, many)]
+    def carries(rows):
+        block = recv_buf.at[pl.ds(0, rows)]
         return pltpu.make_async_remote_copy(
             src_ref=block,
             dst_ref=block,
@@ -164,7 +164,6 @@
     row = lax.broadcasted_iota(jnp.int32, (count, count), 0)
     col = lax.broadcasted_iota(jnp.int32, (count, count), 1)
     gather = jnp.where(col == (row % SUB) * steps + row // SUB, 1.0, 0.0).astype(jnp.bfloat16)
-    scatter = jnp.where(row == (col % SUB) * steps + col // SUB, 1.0, 0.0).astype(jnp.bfloat16)
     sub = lax.broadcasted_iota(jnp.int32, (SUB, block), 0)
 
     def columns(slot):
@@ -272,9 +271,9 @@
             def _():
                 halo_copy.start()
 
-    @pl.when(d > 0)
-    def _():
-        send_halo()
+    with scope("meet_halo"):
+        meet_halo()
+    send_halo()
 
     spread = jnp.broadcast_to(pace_row[...], (LANES, count)).T
     pace_mat[...] = spread
@@ -290,13 +289,6 @@
         for own in range(FIRST, hl):
             for copy in w_copies[own::hl]:
                 copy.start()
-    with scope("meet_halo"):
-        meet_halo()
-
-    @pl.when(d == 0)
-    def _():
-        send_halo()
-
     with scope("own"):
         for slot in range(hl):
             main_slot(slot)
@@ -323,46 +315,65 @@
         def _():
             pl.semaphore_wait(known, 1)
 
-    for rest in range(ROW):
-        for dst in range(nsp - ROW + rest, 0, -ROW):
-
-            @pl.when(me < dst)
-            def _(dst=dst):
-                carry_copy(me, dst).start()
+    planes = -(-nsp // ROW)
+
+    @pl.when(me == 0)
+    def _():
+        for rest in reversed(range(ROW)):
+            for plane in reversed(range(planes)):
+                if 0 < ROW * plane + rest < nsp:
+                    carry_copy(0, ROW * plane + rest, lines).start()
+
+    @pl.when(me > 0)
+    def _():
+        at = lax.rem(me, ROW)
+        for rest in (ROW - 1 - at, at + 1 - 2 * lax.rem(at, 2), lax.rem(at + 2, ROW), at):
+            for plane in reversed(range(planes)):
+                dst = ROW * plane + rest
+
+                @pl.when(jnp.logical_and(me < dst, dst < nsp))
+                def _(dst=dst):
+                    carry_copy(me, dst).start()
+
+    with scope("lay"):
+
+        @pl.loop(0, heads)
+        def _(slot):
+            edge_end = slice(SUB * (EDGE - 1), SUB * EDGE)
+            first_h, first_a = ex_h[slot], ex_a[slot]
+            later_h = hloc[slot, edge_end] + acum[slot, edge_end] * first_h
+            later_a = acum[slot, edge_end] * first_a
+            for j in range(steps):
+                place = slice(SUB * j, SUB * (j + 1))
+                h = hloc[slot, place] + acum[slot, place] * (first_h if j < EDGE else later_h)
+                total_a = acum[slot, place] * (first_a if j < EDGE else later_a)
+                for t in range(tiles):
+                    lanes = slice(LANES * t, LANES * (t + 1))
+                    lay_h[t, place] = h[:, lanes]
+                    lay_a[t, place] = total_a[:, lanes]
+            for t in range(tiles):
+                line = lax.rem(d * hl + slot, heads) * tiles + t
+                for c in range(SUB):
+                    for k in range(0, steps, SUB):
+                        place = slice(steps * c + k, steps * c + k + SUB)
+                        part_h[line, place] = lay_h[t, pl.ds(SUB * k + c, SUB, stride=SUB), :]
+                        part_a[line, place] = lay_a[t, pl.ds(SUB * k + c, SUB, stride=SUB), :]
 
     with scope("carry"):
         for many in range(1, nsp):
 
             @pl.when(me == many)
             def _(many=many):
-                carries(many).wait_recv()
+                carries((2 * many - 1) * lines).wait_recv()
 
     with scope("finish"):
         start = jnp.zeros(carry.shape, jnp.float32)
         for src in range(root):
-            got = recv_buf[src].astype(jnp.float32)
+            got = recv_buf[2 * lines * src : 2 * lines * (src + 1)].astype(jnp.float32)
             start = jnp.exp2(got[:lines]) * start + got[lines:]
-        carry[...] = start
-
         for slot in range(heads):
-            start = jnp.concatenate(
-                [
-                    jnp.broadcast_to(carry[pl.ds(slot * tiles + t, 1), :], (SUB, LANES))
-                    for t in range(tiles)
-                ],
-                axis=1,
-            )
-            start = ex_h[slot] + ex_a[slot] * start
-            edge_end = slice(SUB * (EDGE - 1), SUB * EDGE)
-            later = hloc[slot, edge_end] + acum[slot, edge_end] * start
-            states = [
-                hloc[slot, SUB * j : SUB * (j + 1)]
-                + acum[slot, SUB * j : SUB * (j + 1)] * (start if j < EDGE else later)
-                for j in range(steps)
-            ]
-            states = jnp.concatenate(states, axis=0).astype(jnp.bfloat16)
-            placed = jnp.dot(scatter, states, preferred_element_type=jnp.float32)
-            out_ref[0, :, columns(slot)] = placed.astype(jnp.bfloat16)
+            line = pl.multiple_of(lax.rem(d * hl + slot, heads) * tiles, tiles)
+            carry[pl.ds(line, tiles), :] = start[slot * tiles : (slot + 1) * tiles]
 
     with scope("tail"):
         for copy in w_copies:
@@ -378,7 +389,19 @@
 
             @pl.when(root - me == many)
             def _(many=many):
-                carries(many).wait_send()
+                carries((2 if many < root else 1) * many * lines).wait_send()
+
+
+def finish(part_h, part_a, carry, out_hbm, out, sem):
+    lines = carry.shape[0]
+    count = out.shape[0]
+    for low in range(0, count, 2 * SUB):
+        rows = slice(low, low + 2 * SUB)
+        for line in range(lines):
+            state = part_h[line, rows] + part_a[line, rows] * carry[line : line + 1, :]
+            out[rows, LANES * line : LANES * (line + 1)] = state.astype(jnp.bfloat16)
+        pltpu.make_async_copy(out.at[rows], out_hbm.at[0, rows], sem).start()
+    pltpu.make_async_copy(out, out_hbm.at[0], sem).wait()
 
 
 def body(inputs, conv_weight, gate_weight, rate_param, pace):
@@ -392,11 +415,15 @@
     f32, bf16 = jnp.float32, jnp.bfloat16
     hbm = pl.BlockSpec(memory_space=pltpu.HBM)
     dma = pltpu.SemaphoreType.DMA
-    return pl.pallas_call(
+    part_h, part_a, carry = pl.pallas_call(
         functools.partial(kernel, nsp, ndp, heads, block),
-        out_shape=pltpu.VMEM(inputs.shape, bf16),
+        out_shape=(
+            pltpu.VMEM((lines, count, LANES), f32),
+            pltpu.VMEM((lines, count, LANES), f32),
+            pltpu.VMEM((lines, LANES), f32),
+        ),
         in_specs=[hbm] * 5,
-        out_specs=pl.BlockSpec(memory_space=pltpu.VMEM),
+        out_specs=[pl.BlockSpec(memory_space=pltpu.VMEM)] * 3,
         scratch_shapes=[
             pltpu.VMEM((count, width), bf16),
             pltpu.VMEM(conv_weight.shape, bf16),
@@ -413,10 +440,11 @@
             pltpu.VMEM((heads, count, block), f32),
             pltpu.VMEM((heads, SUB, block), f32),
             pltpu.VMEM((heads, SUB, block), f32),
+            pltpu.VMEM((block // LANES, count, LANES), f32),
+            pltpu.VMEM((block // LANES, count, LANES), f32),
             pltpu.VMEM((2 * lines, LANES), f32),
             pltpu.VMEM((2 * lines, LANES), bf16),
-            pltpu.VMEM((nsp, 2 * lines, LANES), bf16),
-            pltpu.VMEM((lines, LANES), f32),
+            pltpu.VMEM((2 * lines * nsp, LANES), bf16),
             pltpu.SemaphoreType.REGULAR,
             pltpu.SemaphoreType.REGULAR,
             dma,
@@ -430,6 +458,14 @@
         ],
         compiler_params=pltpu.CompilerParams(collective_id=0, has_side_effects=True),
     )(inputs, conv_weight, gate_weight, rate_param.reshape(1, width), pace)
+    return pl.pallas_call(
+        finish,
+        out_shape=jax.ShapeDtypeStruct(inputs.shape, bf16),
+        in_specs=[pl.BlockSpec(memory_space=pltpu.VMEM)] * 3,
+        out_specs=hbm,
+        scratch_shapes=[pltpu.VMEM((count, width), bf16), dma],
+        compiler_params=pltpu.CompilerParams(vmem_limit_bytes=8 * 2**20),
+    )(part_h, part_a, carry)
 
 
 def solution(mesh):

time: 10.9 us -> 10.7 us (0.982)
  local copies, waits for them, and re-layouts: 0.8 us -> 0 us
  Pallas kernels: 9.94 us -> 10.5 us
    pallas_call x0 -> x1, Pallas kernels: none -> 0.81 us  [body(): pl.pallas_call(finish, out_shape=jax.ShapeDtypeStruct(inputs.shape, bf16)...]
    unnamed x1 -> x0, local copies, waits for them, and re-layouts: 0.8 us -> none
    pallas_call x1, Pallas kernels: 9.94 us -> 9.73 us  [body(): pl.pallas_call(functools.partial(kernel, nsp, ndp, heads, block), out_sha...]
where the time goes in v3:
time: 10.7 us; the launch traced here: 10.6 us
  Pallas kernels  10.5 us (98%)
    pallas_call x1, Pallas kernels, body(): pl.pallas_call(functools.partial(kernel, nsp, ndp, heads, block), out_sha...  9.73 us
    pallas_call x1, Pallas kernels, body(): pl.pallas_call(finish, out_shape=jax.ShapeDtypeStruct(inputs.shape, bf16)...  0.81 us

profile of v3, /device:TPU:16, one launch (start us, length us, event | category | flops | bytes accessed | tf_op | source)
XLA Modules:
  0.0 10.6 jit_solution(6225479696178333506)
XLA Ops:
  0.0 9.7 %shard_map.55 = (f32[16,128,128]{2,1,0:T(8,128)S(1)}, f32[16,128,128]{2,1,0:T(8,128)S(1)}, f32[16,128]{1,0:T(8,128)S(1)}) custom-call(bf16[1,128,2048]{2,1,0:T(8,128)(2,1)} %x_hbm.1, bf16[4,2048]{1,0:T(4,128)(2,1)} %cw_hbm.1, bf16[2,4,256,256]{3,2,1,0:T(8,128)(2,1)} %w_hbm.1, f32[1,2048]{1,0:T(1,128)} %bitcast.1, f32[1,2048]{1,0:T(1,128)} %pace_hbm.1), custom_call_target="tpu_custom_call" | custom-call | tf_op jit(solution)/shard_map/pallas_call | solution.py:418
  9.7 0.8 %shard_map.56 = bf16[1,128,2048]{2,1,0:T(8,128)(2,1)} custom-call(f32[16,128,128]{2,1,0:T(8,128)S(1)} %get-tuple-element.8.part_h, f32[16,128,128]{2,1,0:T(8,128)S(1)} %get-tuple-element.9.part_a, f32[16,128]{1,0:T(8,128)S(1)} %get-tuple-element.10.carry), custom_call_target="tpu_custom_call" | custom-call | tf_op jit(solution)/shard_map/pallas_call | solution.py:461

commit v4 on v3

--- a/solution.py
+++ b/solution.py
@@ -32,7 +32,7 @@
     nsp, ndp, heads, block,
     x_hbm, cw_hbm, w_hbm, rate_hbm, pace_hbm, part_h, part_a, carry,
     x, cw, w, rate, pace_row, pace_mat, pace_perm, last, halo,
-    ends, convs, hloc, acum, ex_h, ex_a, lay_h, lay_a, stage, send_buf, recv_buf,
+    convs, conv0, hloc, acum, all_h, all_a, edge_h, edge_a, ex_h, ex_a, lay_h, lay_a, stage, send_buf, recv_buf,
     known, met, load_sem, map_sem, w_send, w_recv, halo_send, halo_recv, c_send, c_recv,
 ):
     me = lax.axis_index("sp")
@@ -43,6 +43,9 @@
     tiles = block // LANES
     lines = heads * tiles
     root = nsp - 1
+    relay = nsp // 2 + 1 if nsp >= 2 * ROW else 0
+    reach = nsp // 2 + ROW - 1
+    near = 2
     scope = jax.named_scope
 
     first = pl.multiple_of(me * count, count)
@@ -86,12 +89,21 @@
         def _():
             greet(root)
 
+    if relay:
+
+        @pl.when(jnp.logical_and(d == 0, (me <= reach) & (me != relay) & (me != relay + 1)))
+        def _():
+            greet(relay)
+
     @pl.when(me == 0)
     def _():
         halo[...] = jnp.zeros_like(halo)
 
     def meet():
-        pl.semaphore_wait(barrier, d + jnp.where(me == root, root if root > 1 else 0, min(root, 1)))
+        expect = jnp.where(me == root, root if root > 1 else 0, min(root, 1))
+        if relay:
+            expect = jnp.where(jnp.logical_and(d == 0, me == relay), reach, expect)
+        pl.semaphore_wait(barrier, d + expect)
 
     def meet_early():
         if root > 0:
@@ -100,7 +112,7 @@
             def _():
                 meet()
                 for there in range(root):
-                    pl.semaphore_signal(known, inc=1, device_id={"sp": there}, device_id_type=MESH)
+                    pl.semaphore_signal(known.at[0], inc=1, device_id={"sp": there}, device_id_type=MESH)
 
     def meet_maps():
         @pl.when(jnp.logical_and(me < max(root, 1), d > 0))
@@ -119,6 +131,13 @@
         @pl.when(jnp.logical_and(me < root, d == 0))
         def _():
             meet()
+
+            if relay:
+
+                @pl.when(me == relay)
+                def _():
+                    for there in range(near):
+                        pl.semaphore_signal(known.at[1], inc=1, device_id={"sp": there}, device_id_type=MESH)
 
     w_copies = []
     for slot in range(hl, heads):
@@ -184,29 +203,19 @@
         here = columns(slot)
         xp = jnp.dot(gather, x[:, here], preferred_element_type=jnp.float32)
         rows = [xp[SUB * j : SUB * (j + 1)] for j in range(steps)]
-        ends[slot] = jnp.concatenate(rows[steps - EDGE :] + rows[:EDGE], axis=0)
+        rows = [pltpu.roll(rows[steps - EDGE + j], 1, 0) for j in range(EDGE)] + rows
         convs[slot] = convolve(rows, here)
 
-    def conv_edge(slot):
-        here = columns(slot)
-        rows = [ends[slot, SUB * j : SUB * (j + 1)] for j in range(2 * EDGE)]
-        before = halo[:, here].astype(jnp.float32)
-        for j in range(EDGE):
-            edge = before[CONV - EDGE + j : CONV - EDGE + j + 1]
-            rows[j] = jnp.where(sub == 0, jnp.broadcast_to(edge, (SUB, block)), pltpu.roll(rows[j], 1, 0))
-        return convolve(rows, here)
-
-    def scan(conv, slot, first_step):
+    def gates(conv, slot, pace_of):
         conv = conv.astype(jnp.bfloat16)
         pre_r = jnp.dot(conv, w[0, slot], preferred_element_type=jnp.float32)
         pre_i = jnp.dot(conv, w[1, slot], preferred_element_type=jnp.float32)
         values = conv.astype(jnp.float32)
         factor = softplus_neg(rate[:, columns(slot)]) * (-gate_power / LN2)
         factor = jnp.broadcast_to(factor, (SUB, block))
-        h = total_a = None
         for j in range(conv.shape[0] // SUB):
             part = slice(SUB * j, SUB * (j + 1))
-            pace_j = jnp.concatenate([pace_perm[first_step + j]] * tiles, axis=1)
+            pace_j = jnp.concatenate([pace_of(j)] * tiles, axis=1)
             r = 1.0 / (1.0 + jnp.exp2(pre_r[part] * -LOG2E))
             i = 1.0 / (1.0 + jnp.exp2(pre_i[part] * -LOG2E))
             n = pace_j * factor * r
@@ -215,35 +224,59 @@
             series = n * (n * (n * (-(c**3) / 6) - c * c / 2) - c)
             gain = jnp.where(n > -SMALL, series, 1.0 - a * a)
             b = gain * lax.rsqrt(jnp.maximum(gain, TINY)) * i * values[part]
-            if h is None:
-                h, total_a = b, a
-            else:
-                h = a * h + b
-                total_a = total_a * a
-            place = slice(SUB * (first_step + j), SUB * (first_step + j + 1))
-            hloc[slot, place] = h
-            acum[slot, place] = total_a
-
-    def main_slot(slot):
-        scan(convs[slot], slot, EDGE)
-
-    def edge_slot(slot):
-        scan(conv_edge(slot), slot, 0)
-        edge_end = slice(SUB * (EDGE - 1), SUB * EDGE)
-        chunk_end = slice(SUB * (steps - 1), SUB * steps)
-        h = hloc[slot, chunk_end] + acum[slot, chunk_end] * hloc[slot, edge_end]
-        totals(slot, h, acum[slot, chunk_end] * acum[slot, edge_end])
-
-    def totals(slot, h, total_a):
-        for shift in (1, 2, 4):
+            yield a, b
+
+    def prefix(h, total_a, shifts):
+        for shift in shifts:
             inside = sub >= shift
             earlier_a = jnp.where(inside, pltpu.roll(total_a, shift, 0), 1.0)
             earlier_h = jnp.where(inside, pltpu.roll(h, shift, 0), 0.0)
             h = total_a * earlier_h + h
             total_a = total_a * earlier_a
-        ex_h[slot] = jnp.where(sub >= 1, pltpu.roll(h, 1, 0), 0.0)
-        ex_a[slot] = jnp.where(sub >= 1, pltpu.roll(total_a, 1, 0), 1.0)
-        log_a = jnp.log2(jnp.maximum(total_a, TINY))
+        return h, total_a
+
+    def main_slot(slot):
+        for j, (a, b) in enumerate(gates(convs[slot], slot, lambda j: pace_perm[j])):
+            if j == 0:
+                h, total_a = b, a
+            elif j == EDGE:
+                h = jnp.where(sub == 0, b, a * h + b)
+                total_a = jnp.where(sub == 0, a, total_a * a)
+            else:
+                h = a * h + b
+                total_a = total_a * a
+            place = slice(SUB * j, SUB * (j + 1))
+            hloc[slot, place] = h
+            acum[slot, place] = total_a
+        h, total_a = prefix(h, total_a, (1, 2, 4))
+        all_h[slot] = h
+        all_a[slot] = total_a
+
+    def conv_edge():
+        own = pltpu.roll(x[:SUB, :].astype(jnp.float32), EDGE, 0)
+        before = jnp.concatenate([halo[...].astype(jnp.float32)] * (SUB // CONV), axis=0)
+        wide = lax.broadcasted_iota(jnp.int32, own.shape, 0)
+        rows = jnp.where(wide < EDGE, before, own)
+        taps = cw[...].astype(jnp.float32)
+        total = taps[0:1] * rows
+        for k in range(1, CONV):
+            total = total + taps[k : k + 1] * pltpu.roll(rows, SUB - k, 0)
+        conv0[...] = total
+
+    def edge_slot(slot):
+        (a, b), = gates(conv0[:, columns(slot)], slot, lambda j: pace_mat[:SUB, :])
+        h, total_a = prefix(b, a, (1, 2))
+        edge_h[slot] = h
+        edge_a[slot] = total_a
+        first_h = jnp.broadcast_to(h[EDGE - 1 : EDGE], (SUB, block))
+        first_a = jnp.broadcast_to(total_a[EDGE - 1 : EDGE], (SUB, block))
+        h, total_a = all_h[slot], all_a[slot]
+        before_h = jnp.where(sub >= 1, pltpu.roll(h, 1, 0), 0.0)
+        before_a = jnp.where(sub >= 1, pltpu.roll(total_a, 1, 0), 1.0)
+        ex_h[slot] = before_h + before_a * first_h
+        ex_a[slot] = before_a * first_a
+        h = h + total_a * first_h
+        log_a = jnp.log2(jnp.maximum(total_a * first_a, TINY))
         for t in range(tiles):
             lanes = slice(LANES * t, LANES * (t + 1))
             stage[pl.ds(slot * tiles + t, 1), :] = log_a[SUB - 1 :, lanes]
@@ -254,7 +287,7 @@
     with scope("loads"):
         for load in loads:
             load.wait()
-    last[...] = x[count - SUB :, :].astype(jnp.float32)[SUB - CONV :].astype(jnp.bfloat16)
+    last[...] = pltpu.roll(x[count - SUB :, :].astype(jnp.float32), EDGE, 0)[:CONV].astype(jnp.bfloat16)
     with scope("meet_maps"):
         meet_maps()
     with scope("maps_a"):
@@ -289,64 +322,98 @@
         for own in range(FIRST, hl):
             for copy in w_copies[own::hl]:
                 copy.start()
-    with scope("own"):
-        for slot in range(hl):
-            main_slot(slot)
-        for slot in range(hl, heads):
-            conv_main(slot)
-    for slot in range(hl, heads):
-        with scope("map%d" % slot):
-            w_copies[slot - hl].wait_recv()
-        with scope("main%d" % slot):
-            main_slot(slot)
-    with scope("take_halo"):
-
-        @pl.when(me > 0)
-        def _():
-            halo_copy.wait_recv()
-
-    with scope("edges"):
-        for slot in range(heads):
-            edge_slot(slot)
-        send_buf[...] = stage[...].astype(jnp.bfloat16)
-    with scope("all_in"):
-
-        @pl.when(me < root)
-        def _():
-            pl.semaphore_wait(known, 1)
-
+    turns = [list(range(hl)), list(range(hl, heads))[:2]] + [[slot] for slot in range(hl + 2, heads)]
+    turns = [turn for turn in turns if turn]
+    for turn, after in zip(turns, turns[1:] + [[]]):
+        if not after:
+            with scope("take_halo"):
+
+                @pl.when(me > 0)
+                def _():
+                    halo_copy.wait_recv()
+
+        with scope("map%d" % turn[0]):
+            for slot in turn:
+                if slot >= hl:
+                    w_copies[slot - hl].wait_recv()
+        with scope("main%d" % turn[0]):
+            for slot in turn:
+                main_slot(slot)
+            for slot in after:
+                conv_main(slot)
+            if not after:
+                conv_edge()
+                for slot in range(heads):
+                    edge_slot(slot)
+                send_buf[...] = stage[...].astype(jnp.bfloat16)
     planes = -(-nsp // ROW)
-
-    @pl.when(me == 0)
-    def _():
+    split = reach // ROW + 1 if relay else 0
+    early = jnp.logical_and(me < near, d == 0) if relay else me < 0
+
+    def all_in():
+        if root > 0:
+
+            @pl.when(me < root)
+            def _():
+                pl.semaphore_wait(known.at[0], 1)
+
+    def send_first(low, high):
         for rest in reversed(range(ROW)):
-            for plane in reversed(range(planes)):
+            for plane in reversed(range(low, high)):
                 if 0 < ROW * plane + rest < nsp:
                     carry_copy(0, ROW * plane + rest, lines).start()
 
-    @pl.when(me > 0)
-    def _():
+    def send_rest(low, high):
         at = lax.rem(me, ROW)
         for rest in (ROW - 1 - at, at + 1 - 2 * lax.rem(at, 2), lax.rem(at + 2, ROW), at):
-            for plane in reversed(range(planes)):
+            for plane in reversed(range(low, high)):
                 dst = ROW * plane + rest
 
                 @pl.when(jnp.logical_and(me < dst, dst < nsp))
                 def _(dst=dst):
                     carry_copy(me, dst).start()
 
+    def send(low, high):
+        @pl.when(me == 0)
+        def _():
+            send_first(low, high)
+
+        @pl.when(me > 0)
+        def _():
+            send_rest(low, high)
+
+    if relay:
+
+        @pl.when(early)
+        def _():
+            pl.semaphore_wait(known.at[1], 1)
+            send(0, split)
+
+    with scope("all_in"):
+        all_in()
+
+    if relay:
+
+        @pl.when(early)
+        def _():
+            send(split, planes)
+
+    @pl.when(jnp.logical_not(early))
+    def _():
+        send(0, planes)
+
     with scope("lay"):
 
         @pl.loop(0, heads)
         def _(slot):
-            edge_end = slice(SUB * (EDGE - 1), SUB * EDGE)
-            first_h, first_a = ex_h[slot], ex_a[slot]
-            later_h = hloc[slot, edge_end] + acum[slot, edge_end] * first_h
-            later_a = acum[slot, edge_end] * first_a
+            before_h, before_a = ex_h[slot], ex_a[slot]
             for j in range(steps):
                 place = slice(SUB * j, SUB * (j + 1))
-                h = hloc[slot, place] + acum[slot, place] * (first_h if j < EDGE else later_h)
-                total_a = acum[slot, place] * (first_a if j < EDGE else later_a)
+                h = hloc[slot, place] + acum[slot, place] * before_h
+                total_a = acum[slot, place] * before_a
+                if j < EDGE:
+                    h = jnp.where(sub == 0, edge_h[slot, j : j + 1], h)
+                    total_a = jnp.where(sub == 0, edge_a[slot, j : j + 1], total_a)
                 for t in range(tiles):
                     lanes = slice(LANES * t, LANES * (t + 1))
                     lay_h[t, place] = h[:, lanes]
@@ -434,10 +501,14 @@
             pltpu.VMEM((count // SUB, SUB, LANES), f32),
             pltpu.VMEM((CONV, width), bf16),
             pltpu.VMEM((CONV, width), bf16),
-            pltpu.VMEM((heads, 2 * EDGE * SUB, block), f32),
-            pltpu.VMEM((heads, count - EDGE * SUB, block), f32),
+            pltpu.VMEM((heads, count, block), f32),
+            pltpu.VMEM((SUB, width), f32),
             pltpu.VMEM((heads, count, block), f32),
             pltpu.VMEM((heads, count, block), f32),
+            pltpu.VMEM((heads, SUB, block), f32),
+            pltpu.VMEM((heads, SUB, block), f32),
+            pltpu.VMEM((heads, SUB, block), f32),
+            pltpu.VMEM((heads, SUB, block), f32),
             pltpu.VMEM((heads, SUB, block), f32),
             pltpu.VMEM((heads, SUB, block), f32),
             pltpu.VMEM((block // LANES, count, LANES), f32),
@@ -445,7 +516,7 @@
             pltpu.VMEM((2 * lines, LANES), f32),
             pltpu.VMEM((2 * lines, LANES), bf16),
             pltpu.VMEM((2 * lines * nsp, LANES), bf16),
-            pltpu.SemaphoreType.REGULAR,
+            pltpu.SemaphoreType.REGULAR((2,)),
             pltpu.SemaphoreType.REGULAR,
             dma,
             dma((2,)),

time: 10.7 us -> 10.6 us (level)
    pallas_call x1, Pallas kernels: 9.73 us -> 9.59 us  [body(): pl.pallas_call(functools.partial(kernel, nsp, ndp, heads, block), out_sha...]
where the time goes in v4:
time: 10.6 us; the launch traced here: 10.4 us
  Pallas kernels  10.4 us (98%)
    pallas_call x1, Pallas kernels, body(): pl.pallas_call(functools.partial(kernel, nsp, ndp, heads, block), out_sha...  9.59 us
    pallas_call x1, Pallas kernels, body(): pl.pallas_call(finish, out_shape=jax.ShapeDtypeStruct(inputs.shape, bf16)...  0.81 us

profile of v4, /device:TPU:16, one launch (start us, length us, event | category | flops | bytes accessed | tf_op | source)
XLA Modules:
  0.0 10.4 jit_solution(2861389918256396639)
XLA Ops:
  0.0 9.6 %shard_map.55 = (f32[16,128,128]{2,1,0:T(8,128)S(1)}, f32[16,128,128]{2,1,0:T(8,128)S(1)}, f32[16,128]{1,0:T(8,128)S(1)}) custom-call(bf16[1,128,2048]{2,1,0:T(8,128)(2,1)} %x_hbm.1, bf16[4,2048]{1,0:T(4,128)(2,1)} %cw_hbm.1, bf16[2,4,256,256]{3,2,1,0:T(8,128)(2,1)} %w_hbm.1, f32[1,2048]{1,0:T(1,128)} %bitcast.1, f32[1,2048]{1,0:T(1,128)} %pace_hbm.1), custom_call_target="tpu_custom_call" | custom-call | tf_op jit(solution)/shard_map/pallas_call | solution.py:485
  9.6 0.8 %shard_map.56 = bf16[1,128,2048]{2,1,0:T(8,128)(2,1)} custom-call(f32[16,128,128]{2,1,0:T(8,128)S(1)} %get-tuple-element.8.part_h, f32[16,128,128]{2,1,0:T(8,128)S(1)} %get-tuple-element.9.part_a, f32[16,128]{1,0:T(8,128)S(1)} %get-tuple-element.10.carry), custom_call_target="tpu_custom_call" | custom-call | tf_op jit(solution)/shard_map/pallas_call | solution.py:532

commit v5 on v4

--- a/solution.py
+++ b/solution.py
@@ -304,17 +304,27 @@
             def _():
                 halo_copy.start()
 
-    with scope("meet_halo"):
-        meet_halo()
-    send_halo()
+    @pl.when(d > 0)
+    def _():
+        send_halo()
 
     spread = jnp.broadcast_to(pace_row[...], (LANES, count)).T
     pace_mat[...] = spread
     for j in range(steps):
         pace_perm[j] = pace_mat[pl.ds(j, SUB, stride=steps), :]
 
-    with scope("conv_own"):
-        for slot in range(hl):
+    with scope("conv_a"):
+        for slot in range(hl // 2):
+            conv_main(slot)
+    with scope("meet_halo"):
+        meet_halo()
+
+    @pl.when(d == 0)
+    def _():
+        send_halo()
+
+    with scope("conv_b"):
+        for slot in range(hl // 2, hl):
             conv_main(slot)
     with scope("maps_b"):
         for load in map_loads[FIRST:]:
@@ -322,30 +332,55 @@
         for own in range(FIRST, hl):
             for copy in w_copies[own::hl]:
                 copy.start()
-    turns = [list(range(hl)), list(range(hl, heads))[:2]] + [[slot] for slot in range(hl + 2, heads)]
-    turns = [turn for turn in turns if turn]
-    for turn, after in zip(turns, turns[1:] + [[]]):
-        if not after:
-            with scope("take_halo"):
-
-                @pl.when(me > 0)
-                def _():
-                    halo_copy.wait_recv()
-
+    def wait_halo():
+        with scope("take_halo"):
+
+            @pl.when(me > 0)
+            def _():
+                halo_copy.wait_recv()
+
+    def wait_maps(turn):
         with scope("map%d" % turn[0]):
             for slot in turn:
                 if slot >= hl:
                     w_copies[slot - hl].wait_recv()
+
+    def mains(turn, after=()):
+        for slot in turn:
+            main_slot(slot)
+        for slot in after:
+            conv_main(slot)
+
+    def edges():
+        conv_edge()
+        for slot in range(heads):
+            edge_slot(slot)
+        send_buf[...] = stage[...].astype(jnp.bfloat16)
+
+    turns = [list(range(hl)), list(range(hl, heads))[:2]] + [[slot] for slot in range(hl + 2, heads)]
+    turns = [turn for turn in turns if turn]
+    for turn, after in zip(turns, turns[1:]):
+        wait_maps(turn)
         with scope("main%d" % turn[0]):
-            for slot in turn:
-                main_slot(slot)
-            for slot in after:
-                conv_main(slot)
-            if not after:
-                conv_edge()
-                for slot in range(heads):
-                    edge_slot(slot)
-                send_buf[...] = stage[...].astype(jnp.bfloat16)
+            mains(turn, after)
+
+    @pl.when(d == 0)
+    def _():
+        wait_maps(turns[-1])
+        with scope("last"):
+            mains(turns[-1])
+        wait_halo()
+        with scope("edges"):
+            edges()
+
+    @pl.when(d > 0)
+    def _():
+        wait_halo()
+        wait_maps(turns[-1])
+        with scope("edges"):
+            mains(turns[-1])
+            edges()
+
     planes = -(-nsp // ROW)
     split = reach // ROW + 1 if relay else 0
     early = jnp.logical_and(me < near, d == 0) if relay else me < 0
@@ -365,7 +400,8 @@
 
     def send_rest(low, high):
         at = lax.rem(me, ROW)
-        for rest in (ROW - 1 - at, at + 1 - 2 * lax.rem(at, 2), lax.rem(at + 2, ROW), at):
+        mid = 1 - lax.rem((at + 1) // 2, 2)
+        for rest in (ROW - 1 - at, mid, ROW - 1 - mid, at):
             for plane in reversed(range(low, high)):
                 dst = ROW * plane + rest
 

time: 10.6 us -> 10.4 us (0.981)
  Pallas kernels: 10.4 us -> 10.2 us
    pallas_call x1, Pallas kernels: 9.59 us -> 9.43 us  [body(): pl.pallas_call(functools.partial(kernel, nsp, ndp, heads, block), out_sha...]
where the time goes in v5:
time: 10.4 us; the launch traced here: 10.3 us
  Pallas kernels  10.2 us (98%)
    pallas_call x1, Pallas kernels, body(): pl.pallas_call(functools.partial(kernel, nsp, ndp, heads, block), out_sha...  9.43 us
    pallas_call x1, Pallas kernels, body(): pl.pallas_call(finish, out_shape=jax.ShapeDtypeStruct(inputs.shape, bf16)...  0.81 us

profile of v5, /device:TPU:16, one launch (start us, length us, event | category | flops | bytes accessed | tf_op | source)
XLA Modules:
  0.0 10.3 jit_solution(10508466257809412085)
XLA Ops:
  0.0 9.4 %shard_map.55 = (f32[16,128,128]{2,1,0:T(8,128)S(1)}, f32[16,128,128]{2,1,0:T(8,128)S(1)}, f32[16,128]{1,0:T(8,128)S(1)}) custom-call(bf16[1,128,2048]{2,1,0:T(8,128)(2,1)} %x_hbm.1, bf16[4,2048]{1,0:T(4,128)(2,1)} %cw_hbm.1, bf16[2,4,256,256]{3,2,1,0:T(8,128)(2,1)} %w_hbm.1, f32[1,2048]{1,0:T(1,128)} %bitcast.1, f32[1,2048]{1,0:T(1,128)} %pace_hbm.1), custom_call_target="tpu_custom_call" | custom-call | tf_op jit(solution)/shard_map/pallas_call | solution.py:521
  9.4 0.8 %shard_map.56 = bf16[1,128,2048]{2,1,0:T(8,128)(2,1)} custom-call(f32[16,128,128]{2,1,0:T(8,128)S(1)} %get-tuple-element.8.part_h, f32[16,128,128]{2,1,0:T(8,128)S(1)} %get-tuple-element.9.part_a, f32[16,128]{1,0:T(8,128)S(1)} %get-tuple-element.10.carry), custom_call_target="tpu_custom_call" | custom-call | tf_op jit(solution)/shard_map/pallas_call | solution.py:568

commit v6 on v5

--- a/solution.py
+++ b/solution.py
@@ -314,7 +314,7 @@
         pace_perm[j] = pace_mat[pl.ds(j, SUB, stride=steps), :]
 
     with scope("conv_a"):
-        for slot in range(hl // 2):
+        for slot in range(hl // 4):
             conv_main(slot)
     with scope("meet_halo"):
         meet_halo()
@@ -324,7 +324,7 @@
         send_halo()
 
     with scope("conv_b"):
-        for slot in range(hl // 2, hl):
+        for slot in range(hl // 4, hl):
             conv_main(slot)
     with scope("maps_b"):
         for load in map_loads[FIRST:]:
@@ -342,8 +342,7 @@
     def wait_maps(turn):
         with scope("map%d" % turn[0]):
             for slot in turn:
-                if slot >= hl:
-                    w_copies[slot - hl].wait_recv()
+                w_copies[slot - hl].wait_recv()
 
     def mains(turn, after=()):
         for slot in turn:
@@ -357,28 +356,34 @@
             edge_slot(slot)
         send_buf[...] = stage[...].astype(jnp.bfloat16)
 
-    turns = [list(range(hl)), list(range(hl, heads))[:2]] + [[slot] for slot in range(hl + 2, heads)]
-    turns = [turn for turn in turns if turn]
-    for turn, after in zip(turns, turns[1:]):
-        wait_maps(turn)
-        with scope("main%d" % turn[0]):
-            mains(turn, after)
+    own, rest = list(range(hl)), list(range(hl, heads))
+    pair, single = rest[:2], [[slot] for slot in rest]
+
+    def run(turns, ahead):
+        for turn, after in zip(turns, ahead):
+            wait_maps(turn)
+            with scope("main%d" % turn[0]):
+                mains(turn, after)
+
+    with scope("main0"):
+        mains(own, pair)
 
     @pl.when(d == 0)
     def _():
-        wait_maps(turns[-1])
-        with scope("last"):
-            mains(turns[-1])
+        run(([pair] if pair else []) + single[2:], single[2:] + [[]])
         wait_halo()
         with scope("edges"):
             edges()
 
     @pl.when(d > 0)
     def _():
+        run(single[:-1], [[]] + single[2:])
         wait_halo()
-        wait_maps(turns[-1])
+        for turn in single[-1:]:
+            wait_maps(turn)
         with scope("edges"):
-            mains(turns[-1])
+            for turn in single[-1:]:
+                mains(turn)
             edges()
 
     planes = -(-nsp // ROW)
@@ -401,8 +406,9 @@
     def send_rest(low, high):
         at = lax.rem(me, ROW)
         mid = 1 - lax.rem((at + 1) // 2, 2)
-        for rest in (ROW - 1 - at, mid, ROW - 1 - mid, at):
-            for plane in reversed(range(low, high)):
+        rests = (ROW - 1 - at, mid, ROW - 1 - mid, at)
+        for rest, way in zip(rests, (-1, 1, 1, -1)):
+            for plane in range(low, high)[::way]:
                 dst = ROW * plane + rest
 
                 @pl.when(jnp.logical_and(me < dst, dst < nsp))
@@ -462,6 +468,22 @@
                         part_h[line, place] = lay_h[t, pl.ds(SUB * k + c, SUB, stride=SUB), :]
                         part_a[line, place] = lay_a[t, pl.ds(SUB * k + c, SUB, stride=SUB), :]
 
+    with scope("sent"):
+        for copy in w_copies:
+            copy.wait_send()
+
+        if root > 0:
+
+            @pl.when(me < root)
+            def _():
+                halo_copy.wait_send()
+
+        for many in range(1, nsp):
+
+            @pl.when(root - me == many)
+            def _(many=many):
+                carries((2 if many < root else 1) * many * lines).wait_send()
+
     with scope("carry"):
         for many in range(1, nsp):
 
@@ -471,28 +493,18 @@
 
     with scope("finish"):
         start = jnp.zeros(carry.shape, jnp.float32)
+        parts = []
         for src in range(root):
             got = recv_buf[2 * lines * src : 2 * lines * (src + 1)].astype(jnp.float32)
-            start = jnp.exp2(got[:lines]) * start + got[lines:]
+            parts.append((jnp.exp2(got[:lines]), got[lines:]))
+        while len(parts) > 1:
+            pairs = [(a0 * a1, a1 * h0 + h1) for (a0, h0), (a1, h1) in zip(parts[::2], parts[1::2])]
+            parts = pairs + parts[len(parts) // 2 * 2 :]
+        if parts:
+            start = parts[0][1]
         for slot in range(heads):
             line = pl.multiple_of(lax.rem(d * hl + slot, heads) * tiles, tiles)
             carry[pl.ds(line, tiles), :] = start[slot * tiles : (slot + 1) * tiles]
-
-    with scope("tail"):
-        for copy in w_copies:
-            copy.wait_send()
-
-        if root > 0:
-
-            @pl.when(me < root)
-            def _():
-                halo_copy.wait_send()
-
-        for many in range(1, nsp):
-
-            @pl.when(root - me == many)
-            def _(many=many):
-                carries((2 if many < root else 1) * many * lines).wait_send()
 
 
 def finish(part_h, part_a, carry, out_hbm, out, sem):

time: 10.4 us -> 10.3 us (level)
    pallas_call x1, Pallas kernels: 9.43 us -> 9.31 us  [body(): pl.pallas_call(functools.partial(kernel, nsp, ndp, heads, block), out_sha...]
where the time goes in v6:
time: 10.3 us; the launch traced here: 10.1 us
  Pallas kernels  10.1 us (98%)
    pallas_call x1, Pallas kernels, body(): pl.pallas_call(functools.partial(kernel, nsp, ndp, heads, block), out_sha...  9.31 us
    pallas_call x1, Pallas kernels, body(): pl.pallas_call(finish, out_shape=jax.ShapeDtypeStruct(inputs.shape, bf16)...  0.81 us

profile of v6, /device:TPU:16, one launch (start us, length us, event | category | flops | bytes accessed | tf_op | source)
XLA Modules:
  0.0 10.1 jit_solution(14806353316167614013)
XLA Ops:
  0.0 9.3 %shard_map.55 = (f32[16,128,128]{2,1,0:T(8,128)S(1)}, f32[16,128,128]{2,1,0:T(8,128)S(1)}, f32[16,128]{1,0:T(8,128)S(1)}) custom-call(bf16[1,128,2048]{2,1,0:T(8,128)(2,1)} %x_hbm.1, bf16[4,2048]{1,0:T(4,128)(2,1)} %cw_hbm.1, bf16[2,4,256,256]{3,2,1,0:T(8,128)(2,1)} %w_hbm.1, f32[1,2048]{1,0:T(1,128)} %bitcast.1, f32[1,2048]{1,0:T(1,128)} %pace_hbm.1), custom_call_target="tpu_custom_call" | custom-call | tf_op jit(solution)/shard_map/pallas_call | solution.py:533
  9.3 0.8 %shard_map.56 = bf16[1,128,2048]{2,1,0:T(8,128)(2,1)} custom-call(f32[16,128,128]{2,1,0:T(8,128)S(1)} %get-tuple-element.8.part_h, f32[16,128,128]{2,1,0:T(8,128)S(1)} %get-tuple-element.9.part_a, f32[16,128]{1,0:T(8,128)S(1)} %get-tuple-element.10.carry), custom_call_target="tpu_custom_call" | custom-call | tf_op jit(solution)/shard_map/pallas_call | solution.py:580

commit v7 on v6

--- a/solution.py
+++ b/solution.py
@@ -31,9 +31,9 @@
 def kernel(
     nsp, ndp, heads, block,
     x_hbm, cw_hbm, w_hbm, rate_hbm, pace_hbm, part_h, part_a, carry,
-    x, cw, w, rate, pace_row, pace_mat, pace_perm, last, halo,
+    x, cw, w, rate, factors, pace_row, pace_mat, pace_perm, last, halo,
     convs, conv0, hloc, acum, all_h, all_a, edge_h, edge_a, ex_h, ex_a, lay_h, lay_a, stage, send_buf, recv_buf,
-    known, met, load_sem, map_sem, w_send, w_recv, halo_send, halo_recv, c_send, c_recv,
+    known, met, load_sem, map_sem, sent, w_recv, halo_recv, c_recv,
 ):
     me = lax.axis_index("sp")
     d = lax.axis_index("dp")
@@ -145,7 +145,7 @@
         w_copies.append(pltpu.make_async_remote_copy(
             src_ref=w.at[:, own],
             dst_ref=w.at[:, slot],
-            send_sem=w_send,
+            send_sem=sent,
             recv_sem=w_recv.at[slot - hl],
             device_id={"dp": lax.rem(d - o + ndp, ndp)},
             device_id_type=MESH,
@@ -153,7 +153,7 @@
     halo_copy = pltpu.make_async_remote_copy(
         src_ref=last,
         dst_ref=halo,
-        send_sem=halo_send,
+        send_sem=sent,
         recv_sem=halo_recv,
         device_id={"sp": lax.rem(me + 1, nsp)},
         device_id_type=MESH,
@@ -163,7 +163,7 @@
         return pltpu.make_async_remote_copy(
             src_ref=send_buf.at[pl.ds(low, 2 * lines - low)],
             dst_ref=recv_buf.at[pl.ds(2 * lines * src + low, 2 * lines - low)],
-            send_sem=c_send,
+            send_sem=sent,
             recv_sem=c_recv,
             device_id={"sp": dst},
             device_id_type=MESH,
@@ -174,7 +174,7 @@
         return pltpu.make_async_remote_copy(
             src_ref=block,
             dst_ref=block,
-            send_sem=c_send,
+            send_sem=sent,
             recv_sem=c_recv,
             device_id={"sp": root - me},
             device_id_type=MESH,
@@ -211,8 +211,11 @@
         pre_r = jnp.dot(conv, w[0, slot], preferred_element_type=jnp.float32)
         pre_i = jnp.dot(conv, w[1, slot], preferred_element_type=jnp.float32)
         values = conv.astype(jnp.float32)
-        factor = softplus_neg(rate[:, columns(slot)]) * (-gate_power / LN2)
-        factor = jnp.broadcast_to(factor, (SUB, block))
+        line = lax.rem(d * hl + slot, heads) * tiles
+        factor = jnp.concatenate(
+            [jnp.broadcast_to(factors[pl.ds(line + t, 1), :], (SUB, LANES)) for t in range(tiles)],
+            axis=1,
+        )
         for j in range(conv.shape[0] // SUB):
             part = slice(SUB * j, SUB * (j + 1))
             pace_j = jnp.concatenate([pace_of(j)] * tiles, axis=1)
@@ -308,6 +311,7 @@
     def _():
         send_halo()
 
+    factors[...] = softplus_neg(rate[...]) * (-gate_power / LN2)
     spread = jnp.broadcast_to(pace_row[...], (LANES, count)).T
     pace_mat[...] = spread
     for j in range(steps):
@@ -543,7 +547,8 @@
             pltpu.VMEM((count, width), bf16),
             pltpu.VMEM(conv_weight.shape, bf16),
             pltpu.VMEM((2, heads, block, block), bf16),
-            pltpu.VMEM((1, width), f32),
+            pltpu.VMEM((lines, LANES), f32),
+            pltpu.VMEM((lines, LANES), f32),
             pltpu.VMEM((1, count), f32),
             pltpu.VMEM((count, LANES), f32),
             pltpu.VMEM((count // SUB, SUB, LANES), f32),
@@ -572,11 +577,9 @@
             dma((heads - hl,)),
             dma,
             dma,
-            dma,
-            dma,
         ],
         compiler_params=pltpu.CompilerParams(collective_id=0, has_side_effects=True),
-    )(inputs, conv_weight, gate_weight, rate_param.reshape(1, width), pace)
+    )(inputs, conv_weight, gate_weight, rate_param.reshape(lines, LANES), pace)
     return pl.pallas_call(
         finish,
         out_shape=jax.ShapeDtypeStruct(inputs.shape, bf16),

time: 10.3 us -> 10.3 us (level)
  no operation moved by 1% of the time
where the time goes in v7:
time: 10.3 us; the launch traced here: 10.1 us
  Pallas kernels  10.1 us (98%)
    pallas_call x1, Pallas kernels, body(): pl.pallas_call(functools.partial(kernel, nsp, ndp, heads, block), out_sha...  9.29 us
    pallas_call x1, Pallas kernels, body(): pl.pallas_call(finish, out_shape=jax.ShapeDtypeStruct(inputs.shape, bf16)...  0.81 us

profile of v7, /device:TPU:16, one launch (start us, length us, event | category | flops | bytes accessed | tf_op | source)
XLA Modules:
  0.0 10.1 jit_solution(9264560846361702661)
XLA Ops:
  0.0 9.3 %shard_map.55 = (f32[16,128,128]{2,1,0:T(8,128)S(1)}, f32[16,128,128]{2,1,0:T(8,128)S(1)}, f32[16,128]{1,0:T(8,128)S(1)}) custom-call(bf16[1,128,2048]{2,1,0:T(8,128)(2,1)} %x_hbm.1, bf16[4,2048]{1,0:T(4,128)(2,1)} %cw_hbm.1, bf16[2,4,256,256]{3,2,1,0:T(8,128)(2,1)} %w_hbm.1, f32[16,128]{1,0:T(8,128)} %bitcast.1, f32[1,2048]{1,0:T(1,128)} %pace_hbm.1), custom_call_target="tpu_custom_call" | custom-call | tf_op jit(solution)/shard_map/pallas_call | solution.py:537
  9.3 0.8 %shard_map.56 = bf16[1,128,2048]{2,1,0:T(8,128)(2,1)} custom-call(f32[16,128,128]{2,1,0:T(8,128)S(1)} %get-tuple-element.8.part_h, f32[16,128,128]{2,1,0:T(8,128)S(1)} %get-tuple-element.9.part_a, f32[16,128]{1,0:T(8,128)S(1)} %get-tuple-element.10.carry), custom_call_target="tpu_custom_call" | custom-call | tf_op jit(solution)/shard_map/pallas_call | solution.py:583

commit v8 on v7

--- a/solution.py
+++ b/solution.py
@@ -411,7 +411,7 @@
         at = lax.rem(me, ROW)
         mid = 1 - lax.rem((at + 1) // 2, 2)
         rests = (ROW - 1 - at, mid, ROW - 1 - mid, at)
-        for rest, way in zip(rests, (-1, 1, 1, -1)):
+        for rest, way in zip(rests, (-1, 1, 1, 1)):
             for plane in range(low, high)[::way]:
                 dst = ROW * plane + rest
 

time: 10.3 us -> 10.2 us (level)
  no operation moved by 1% of the time
where the time goes in v8:
time: 10.2 us; the launch traced here: 10.1 us
  Pallas kernels  10 us (98%)
    pallas_call x1, Pallas kernels, body(): pl.pallas_call(functools.partial(kernel, nsp, ndp, heads, block), out_sha...  9.23 us
    pallas_call x1, Pallas kernels, body(): pl.pallas_call(finish, out_shape=jax.ShapeDtypeStruct(inputs.shape, bf16)...  0.81 us

profile of v8, /device:TPU:16, one launch (start us, length us, event | category | flops | bytes accessed | tf_op | source)
XLA Modules:
  0.0 10.1 jit_solution(10289730999032758889)
XLA Ops:
  0.0 9.2 %shard_map.55 = (f32[16,128,128]{2,1,0:T(8,128)S(1)}, f32[16,128,128]{2,1,0:T(8,128)S(1)}, f32[16,128]{1,0:T(8,128)S(1)}) custom-call(bf16[1,128,2048]{2,1,0:T(8,128)(2,1)} %x_hbm.1, bf16[4,2048]{1,0:T(4,128)(2,1)} %cw_hbm.1, bf16[2,4,256,256]{3,2,1,0:T(8,128)(2,1)} %w_hbm.1, f32[16,128]{1,0:T(8,128)} %bitcast.1, f32[1,2048]{1,0:T(1,128)} %pace_hbm.1), custom_call_target="tpu_custom_call" | custom-call | tf_op jit(solution)/shard_map/pallas_call | solution.py:537
  9.2 0.8 %shard_map.56 = bf16[1,128,2048]{2,1,0:T(8,128)(2,1)} custom-call(f32[16,128,128]{2,1,0:T(8,128)S(1)} %get-tuple-element.8.part_h, f32[16,128,128]{2,1,0:T(8,128)S(1)} %get-tuple-element.9.part_a, f32[16,128]{1,0:T(8,128)S(1)} %get-tuple-element.10.carry), custom_call_target="tpu_custom_call" | custom-call | tf_op jit(solution)/shard_map/pallas_call | solution.py:583

commit v9 on v8

--- a/solution.py
+++ b/solution.py
@@ -59,7 +59,7 @@
         pltpu.make_async_copy(w_hbm.at[:, own], w.at[:, own], map_sem.at[int(own >= FIRST)])
         for own in range(hl)
     ]
-    for load in loads + map_loads:
+    for load in loads[:1] + map_loads[:FIRST]:
         load.start()
 
     recv_buf[...] = jnp.zeros_like(recv_buf)
@@ -94,6 +94,9 @@
         @pl.when(jnp.logical_and(d == 0, (me <= reach) & (me != relay) & (me != relay + 1)))
         def _():
             greet(relay)
+
+    for load in loads[1:] + map_loads[FIRST:]:
+        load.start()
 
     @pl.when(me == 0)
     def _():

time: 10.2 us -> 10.2 us (level)
  no operation moved by 1% of the time
where the time goes in v9:
time: 10.2 us; the launch traced here: 10.1 us
  Pallas kernels  10.1 us (99%)
    pallas_call x1, Pallas kernels, body(): pl.pallas_call(functools.partial(kernel, nsp, ndp, heads, block), out_sha...  9.28 us
    pallas_call x1, Pallas kernels, body(): pl.pallas_call(finish, out_shape=jax.ShapeDtypeStruct(inputs.shape, bf16)...  0.81 us

profile of v9, /device:TPU:16, one launch (start us, length us, event | category | flops | bytes accessed | tf_op | source)
XLA Modules:
  0.0 10.1 jit_solution(8302596678594111762)
XLA Ops:
  0.0 9.3 %shard_map.55 = (f32[16,128,128]{2,1,0:T(8,128)S(1)}, f32[16,128,128]{2,1,0:T(8,128)S(1)}, f32[16,128]{1,0:T(8,128)S(1)}) custom-call(bf16[1,128,2048]{2,1,0:T(8,128)(2,1)} %x_hbm.1, bf16[4,2048]{1,0:T(4,128)(2,1)} %cw_hbm.1, bf16[2,4,256,256]{3,2,1,0:T(8,128)(2,1)} %w_hbm.1, f32[16,128]{1,0:T(8,128)} %bitcast.1, f32[1,2048]{1,0:T(1,128)} %pace_hbm.1), custom_call_target="tpu_custom_call" | custom-call | tf_op jit(solution)/shard_map/pallas_call | solution.py:540
  9.3 0.8 %shard_map.56 = bf16[1,128,2048]{2,1,0:T(8,128)(2,1)} custom-call(f32[16,128,128]{2,1,0:T(8,128)S(1)} %get-tuple-element.8.part_h, f32[16,128,128]{2,1,0:T(8,128)S(1)} %get-tuple-element.9.part_a, f32[16,128]{1,0:T(8,128)S(1)} %get-tuple-element.10.carry), custom_call_target="tpu_custom_call" | custom-call | tf_op jit(solution)/shard_map/pallas_call | solution.py:586
